TPU v7x, 128 devices: a whole 4x4x4 slice. The times are simulated.
128 devices in a mesh: sp: 16 (over z, y), tp: 8 (over x, core).
Axes of the slice: x: 4, y: 4, z: 4, core: 2. Of those that a mesh axis runs over, the one named last changes fastest.
Arguments:
- resid: bfloat16 [6144, 2048], P('sp', 'tp'), may hold values from -6 to 6
- mixer_in: bfloat16 [6144, 2048], P('sp', 'tp'), may hold values from -6 to 6
- log_step: float32 [6144, 128], P('sp', 'tp'), may hold values from -5.2 to -0.79
- decay_real: float32 [128, 64], P('tp'), may hold values from 8.138021e-05 to 0.8
- frequency: float32 [128, 64], P('tp'), may hold values from 0.5 to 6
- input_matrix: float32 [2, 128, 64, 16], P(None, 'tp'), may hold values from -1 to 1
- output_matrix: float32 [2, 128, 16, 64], P(None, 'tp'), may hold values from -0.5 to 0.5
- skip_gain: float32 [2048], P('tp'), may hold values from -4 to 4
- value_weight: bfloat16 [2048, 2048], P(None, 'tp'), may hold values from -0.125 to 0.125
- gate_weight: bfloat16 [2048, 2048], P(None, 'tp'), may hold values from -0.125 to 0.125
- norm_gain: float32 [2048], replicated, may hold values from 0.1 to 1.9
- up_weight: bfloat16 [2048, 8192], P('sp', 'tp'), may hold values from -0.125 to 0.125
- down_weight: bfloat16 [2048, 8192], P('sp', 'tp'), may hold values from -0.0625 to 0.0625
Outputs:
- result: bfloat16 [6144, 2048], P('sp', 'tp')
All inputs are finite; a program needn't handle non-finite values.
Results may differ from a plain program's by a relative error of at most 0.014.
Values may be sent and summed in bfloat16 or wider, within the bound.
A program may use at most 128 MiB of HBM per device.

v0:
```python
import jax
import jax.numpy as jnp
from jax import lax
from jax.sharding import PartitionSpec as P

rms_eps = 1e-06


def in_one_piece(arrays, axis, dim, along):
    widths = [a.shape[along] for a in arrays]
    both = jnp.concatenate(arrays, axis=along)
    whole = lax.all_gather(both, axis, axis=dim, tiled=True)
    return tuple(jnp.split(whole, [sum(widths[:k]) for k in range(1, len(widths))], axis=along))


def sent_to_all(value, axis):
    copies = jnp.broadcast_to(value, (lax.axis_size(axis), *value.shape))
    return lax.all_to_all(copies, axis, split_axis=0, concat_axis=0, tiled=True)


def collected_together(value, axis):
    leaves = jax.tree.leaves(value)
    order = sorted(range(len(leaves)), key=lambda k: -leaves[k].size)
    width = (1, *leaves[order[0]].shape)[-1]
    lines = [
        jnp.pad(leaves[k].reshape(-1), (0, -leaves[k].size % width)).reshape(-1, width)
        for k in order
    ]
    both, at, found = (sent_to_all(jnp.concatenate(lines), axis), 0, {})
    for k, line in zip(order, lines):
        section = both[:, at : at + len(line)].reshape(len(both), -1)
        found[k] = section[:, : leaves[k].size].reshape(-1, *leaves[k].shape)
        at += len(line)
    numbers = iter(range(len(leaves)))
    return jax.tree.map(lambda _: found[next(numbers)], value)


def folded_in_pairs(pieces, combine):
    while len(jax.tree.leaves(pieces)[0]) > 1:
        pieces = jax.vmap(combine)(
            *(jax.tree.map(lambda part: part[side::2], pieces) for side in (0, 1))
        )
    return jax.tree.map(lambda part: part[0], pieces)


def prefix(value, axis, combine, identity):
    devices, here = (lax.axis_size(axis), lax.axis_index(axis))
    passed = jnp.arange(devices) < here

    def kept(part, zero, own):
        part = jnp.where(
            passed.reshape(-1, *(1 for _ in own.shape)), part, jnp.asarray(zero, own.dtype)
        )
        return part

    pieces = collected_together(value, axis)
    return folded_in_pairs(jax.tree.map(kept, pieces, identity, value), combine)


def in_order(pieces, dim):
    pieces = jnp.moveaxis(pieces, 0, dim)
    lengths = pieces.shape
    return pieces.reshape(*lengths[:dim], lengths[dim] * lengths[dim + 1], *lengths[dim + 2 :])


def gather_directly(value, axis, dim):
    pieces = sent_to_all(value, axis)
    return in_order(pieces, dim)


def split_up(value, dim, devices):
    lengths = value.shape
    pieces = value.reshape(*lengths[:dim], devices, lengths[dim] // devices, *lengths[dim + 1 :])
    return jnp.moveaxis(pieces, dim, 0)


def sent_and_summed(value, axis, dim):
    pieces = split_up(value, dim, lax.axis_size(axis))
    arrived = lax.all_to_all(pieces, axis, split_axis=0, concat_axis=0, tiled=True)
    return arrived.astype(jnp.float32).sum(axis=0)


def chain_link(earlier, later):
    return (
        earlier[0] * later[0] - earlier[1] * later[1],
        earlier[0] * later[1] + earlier[1] * later[0],
        later[0] * earlier[2] - later[1] * earlier[3] + later[2],
        later[0] * earlier[3] + later[1] * earlier[2] + later[3],
    )


def discretize(log_step, decay_real, frequency):
    states = decay_real.shape[1]
    step_size = jnp.repeat(jnp.exp(log_step), states, axis=1)
    decay_rate = decay_real.reshape(-1)
    angular = frequency.reshape(-1)
    shrink = -decay_rate * step_size
    rotation = angular * step_size
    factor = jnp.exp(shrink)
    decay_re = factor * jnp.cos(rotation)
    decay_im = factor * jnp.sin(rotation)
    half_sine = jnp.sin(0.5 * rotation)
    minus_re = jnp.expm1(shrink) * jnp.cos(rotation) - 2.0 * half_sine * half_sine
    modulus = decay_rate * decay_rate + angular * angular
    drive_re = (decay_im * angular - minus_re * decay_rate) / modulus
    drive_im = (-decay_im * decay_rate - minus_re * angular) / modulus
    return (decay_re, decay_im, drive_re, drive_im)


def local_states(mixer_in, log_step, decay_real, frequency, input_matrix):
    tokens = mixer_in.shape[0]
    groups, states = decay_real.shape
    signal = mixer_in.astype(jnp.float32).reshape(tokens, groups, -1)
    proj_re = jnp.einsum("tgk,gnk->tgn", signal, input_matrix[0]).reshape(tokens, groups * states)
    proj_im = jnp.einsum("tgk,gnk->tgn", signal, input_matrix[1]).reshape(tokens, groups * states)
    decay_re, decay_im, drive_re, drive_im = discretize(log_step, decay_real, frequency)
    feed_re = drive_re * proj_re - drive_im * proj_im
    feed_im = drive_re * proj_im + drive_im * proj_re
    chain_rows = lax.associative_scan(chain_link, (decay_re, decay_im, feed_re, feed_im), axis=0)
    end_states = tuple((member[-1] for member in chain_rows))
    return (end_states, chain_rows)


def read_out(state_re, state_im, output_matrix):
    tokens = state_re.shape[0]
    groups = output_matrix.shape[1]
    grid_re = state_re.reshape(tokens, groups, -1)
    grid_im = state_im.reshape(tokens, groups, -1)
    output = jnp.einsum("tgn,gkn->tgk", grid_re, output_matrix[0])
    output = output - jnp.einsum("tgn,gkn->tgk", grid_im, output_matrix[1])
    return output.reshape(tokens, -1)


def per_device(
    resid,
    mixer_in,
    log_step,
    decay_real,
    frequency,
    input_matrix,
    output_matrix,
    skip_gain,
    value_weight,
    gate_weight,
    norm_gain,
    up_weight,
    down_weight,
):
    up_whole, down_whole = in_one_piece((up_weight, down_weight), "sp", 0, 1)
    end_states, chain_rows = local_states(mixer_in, log_step, decay_real, frequency, input_matrix)
    cum_re, cum_im, part_re, part_im = chain_rows
    zero_state = jnp.zeros_like(end_states[0])
    identity_state = (jnp.ones_like(end_states[0]), zero_state, zero_state, zero_state)
    _, _, carry_re, carry_im = prefix(end_states, "sp", chain_link, identity_state)
    state_re = part_re + cum_re * carry_re - cum_im * carry_im
    state_im = part_im + cum_re * carry_im + cum_im * carry_re
    mechanism = read_out(state_re, state_im, output_matrix) + skip_gain * mixer_in.astype(
        jnp.float32
    )
    mixed_out = jax.nn.gelu(mechanism).astype(jnp.bfloat16)
    channels = gather_directly(mixed_out, "tp", 1)
    value_pre = jnp.dot(channels, value_weight, preferred_element_type=jnp.float32)
    gate_pre = jnp.dot(channels, gate_weight, preferred_element_type=jnp.float32)
    updated = (resid.astype(jnp.float32) + value_pre * jax.nn.sigmoid(gate_pre)).astype(
        jnp.bfloat16
    )
    updated_wide = lax.optimization_barrier(updated).astype(jnp.float32)
    whole_rows = gather_directly(updated, "tp", 1).astype(jnp.float32)
    inv_rms = lax.rsqrt(jnp.mean(whole_rows * whole_rows, axis=1, keepdims=True) + rms_eps)
    normed = (whole_rows * inv_rms * norm_gain).astype(jnp.bfloat16)
    raised = jnp.dot(normed, up_whole, preferred_element_type=jnp.float32)
    active = jax.nn.relu(raised)
    hidden = (active * active).astype(jnp.bfloat16)
    partials = lax.dot_general(
        hidden, down_whole, (((1,), (1,)), ((), ())), preferred_element_type=jnp.float32
    )
    down_sum = sent_and_summed(partials.astype(jnp.bfloat16), "tp", 1)
    return (updated_wide + down_sum).astype(jnp.bfloat16)


def solution(mesh):
    in_specs = (
        P("sp", "tp"),
        P("sp", "tp"),
        P("sp", "tp"),
        P("tp", None),
        P("tp", None),
        P(None, "tp", None, None),
        P(None, "tp", None, None),
        P("tp"),
        P(None, "tp"),
        P(None, "tp"),
        P(),
        P("sp", "tp"),
        P("sp", "tp"),
    )
    out_specs = P("sp", "tp")
    return jax.shard_map(
        per_device, mesh=mesh, in_specs=in_specs, out_specs=out_specs, check_vma=False
    )
```

profile of v0, /device:TPU:1, one launch (start us, length us, event | category | flops | bytes accessed | tf_op | source)
XLA Modules:
  0.0 440.8 jit_solution(10775297982641135820)
XLA Ops:
  6.5 2.0 pad_maximum_fusion.4
  10.9 3.1 copy.205
  17.4 14.7 %multiply_add_fusion.1 = (f32[384,1024]{1,0:T(8,128)S(1)}, f32[384,1024]{1,0:T(8,128)}, f32[384,1024]{1,0:T(8,128)}, f32[384,1024]{1,0:T(8,128)}) fusion(f32[384,1024]{1,0:T(8,128)} %copy.205, f32[384,1024]{1,0:T(8,128)} %copy.206, f32[1024]{0:T(1024)S(1)} %get-tuple-element.114, f32[1024]{0:T(1024)S(1)} %reshape.86, f32[384,1024]{1,0:T(8,128)} %copy.202, ...), kind=kLoop, calls=%fused_computation.16 | loop fusion | flops 9437184 | bytes 11026432 | tf_op jit(solution)/shard_map/add | solution.py:118
  32.1 4.4 slice.609
  36.4 4.3 slice.612
  40.8 4.4 slice.608
  45.1 4.4 slice.614
  49.5 4.3 slice.610
  53.9 4.4 slice.615
  58.2 2.2 slice.611
  60.4 2.1 slice.620
  62.5 5.2 %multiply_subtract_fusion.3 = (f32[192,1024]{1,0:T(8,128)}, f32[192,1024]{1,0:T(8,128)}, f32[192,1024]{1,0:T(8,128)S(1)}, f32[192,1024]{1,0:T(8,128)}) fusion(f32[192,1024]{1,0:T(8,128)} %slice.615, f32[192,1024]{1,0:T(8,128)} %slice.610, f32[192,1024]{1,0:T(8,128)} %slice.614, f32[192,1024]{1,0:T(8,128)} %slice.608, f32[192,1024]{1,0:T(8,128)} %slice.612, ...), kind=kLoop, calls=%fused_computation.46 | loop fusion | flops 2752512 | bytes 9437184 | tf_op jit(solution)/shard_map/sub | solution.py:85
  70.5 2.7 slice.617
  73.2 2.7 slice.624
  76.0 2.7 slice.619
  78.7 2.7 slice.625
  81.4 2.7 slice.621
  84.1 2.7 slice.630
  86.8 3.4 add_add_fusion.3
  103.6 2.4 multiply_subtract_fusion.7
  118.7 2.0 add_add_fusion.7
  183.7 2.8 slice.616
  186.5 2.7 slice.715
  191.9 4.4 %slice.607 = f32[191,1024]{1,0:T(8,128)} slice(f32[384,1024]{1,0:T(8,128)} %get-tuple-element.31), slice={[2:384:2], [0:1024:1]} | slice | bytes 1564672 | tf_op jit(solution)/shard_map/slice | solution.py:119
  196.3 4.4 %slice.721 = f32[191,1024]{1,0:T(8,128)} slice(f32[384,1024]{1,0:T(8,128)} %get-tuple-element.30), slice={[2:384:2], [0:1024:1]} | slice | bytes 1564672 | tf_op jit(solution)/shard_map/slice | solution.py:119
  232.1 2.7 slice.723
  236.9 4.5 %slice.725 = f32[191,1024]{1,0:T(8,128)} slice(f32[384,1024]{1,0:T(8,128)} %get-tuple-element.17), slice={[2:384:2], [0:1024:1]} | slice | bytes 1564672 | tf_op jit(solution)/shard_map/slice | solution.py:119
  241.4 2.3 slice.760
  255.4 1.8 pad_maximum_fusion.8
  257.2 2.9 pad.252
  264.7 3.1 pad.254
  267.9 3.1 pad.255
  271.1 3.3 pad.256
  274.6 3.2 pad.257
  289.7 2.9 pad.221
  292.6 2.2 add.573
  298.5 3.2 pad.224
  301.7 3.1 pad.225
  304.8 3.1 pad.259
  308.1 3.2 pad.258
  315.2 8.6 %all-to-all-start = ((f32[16,4,1024]{2,1,0:T(4,128)}), f32[16,4,1024]{2,1,0:T(4,128)S(1)}, u32[]{:S(2)}, u32[]{:S(2)}) async-start(f32[16,4,1024]{2,1,0:T(4,128)} %broadcast_in_dim.48), calls=%async_computation | async-start | bytes 524288 | tf_op jit(solution)/shard_map/all_to_all | solution.py:18
  323.9 7.5 %all-to-all-done = f32[16,4,1024]{2,1,0:T(4,128)S(1)} async-done(((f32[16,4,1024]{2,1,0:T(4,128)}), f32[16,4,1024]{2,1,0:T(4,128)S(1)}, u32[]{:S(2)}, u32[]{:S(2)}) %all-to-all-start) | async-done | bytes 262176 | tf_op jit(solution)/shard_map/all_to_all | solution.py:18
  332.4 6.7 %multiply_add_fusion = (bf16[384,1024]{1,0:T(8,128)(2,1)S(1)}, bf16[384,1024]{1,0:T(8,128)(2,1)}) fusion(f32[384,1024]{1,0:T(8,128)} %pad.258, f32[384,1024]{1,0:T(8,128)} %pad.259, f32[1024]{0:T(1024)S(1)} %bitcast.80, f32[1024]{0:T(1024)S(1)} %bitcast.79, f32[384,1024]{1,0:T(8,128)} %pad.256, f32[384,1024]{1,0:T(8,128)} %pad.257, ...), kind=kLoop, calls=%fused_computation.14 | loop fusion | flops 5505024 | bytes 14163968 | tf_op jit(solution)/shard_map/add | solution.py:156
  344.0 26.7 %all_to_all.20 = bf16[8,384,256]{1,2,0:T(8,128)(2,1)S(1)} all-to-all(bf16[8,384,256]{1,2,0:T(8,128)(2,1)S(1)} %broadcast_in_dim.51), channel_id=1, replica_groups=mesh['sp'=16,'tp'=8] {'tp'}, dimensions={0} | all-to-all | bytes 3145728 | tf_op jit(solution)/shard_map/all_to_all | solution.py:18
  373.0 24.0 %all_to_all.21 = bf16[8,384,256]{1,2,0:T(8,128)(2,1)S(1)} all-to-all(bf16[8,384,256]{1,2,0:T(8,128)(2,1)S(1)} %broadcast_in_dim.52), channel_id=1, replica_groups=mesh['sp'=16,'tp'=8] {'tp'}, dimensions={0} | all-to-all | bytes 3145728 | tf_op jit(solution)/shard_map/all_to_all | solution.py:18
  399.3 7.3 %fusion.6 = bf16[384,2048]{1,0:T(8,128)(2,1)S(1)} fusion(bf16[2048,2048]{1,0:T(8,128)(2,1)} %all-gather.2.cloned.1.call-done, bf16[384,2048]{0,1:T(8,128)(2,1)} %fusion.5), kind=kOutput, calls=%fused_computation.9 | convolution fusion | flops 3223191552 | bytes 11534336 | tf_op jit(solution)/shard_map/dot_general | solution.py:174
  407.9 4.5 %all-to-all-start.3 = ((bf16[8,384,256]{2,1,0:T(8,128)(2,1)}), bf16[8,384,256]{2,1,0:T(8,128)(2,1)S(1)}, u32[]{:S(2)}, u32[]{:S(2)}) async-start(bf16[8,384,256]{2,1,0:T(8,128)(2,1)} %bitcast.67), calls=%async_computation.3 | async-start | bytes 3145728 | tf_op jit(solution)/shard_map/all_to_all | solution.py:79
  412.4 20.6 %all-to-all-done.3 = bf16[8,384,256]{2,1,0:T(8,128)(2,1)S(1)} async-done(((bf16[8,384,256]{2,1,0:T(8,128)(2,1)}), bf16[8,384,256]{2,1,0:T(8,128)(2,1)S(1)}, u32[]{:S(2)}, u32[]{:S(2)}) %all-to-all-start.3) | async-done | bytes 1572896 | tf_op jit(solution)/shard_map/all_to_all | solution.py:79
  (494 shorter events, 180.7 us)
Async XLA Ops:
  6.5 364.2 %copy-start = (bf16[2048,256]{1,0:T(8,128)(2,1)S(1)}, bf16[2048,256]{1,0:T(8,128)(2,1)}, u32[]{:S(2)}) copy-start(bf16[2048,256]{1,0:T(8,128)(2,1)} %param.22) | copy-start | bytes 3145732
  6.5 392.7 %all-gather.2.cloned.1.call-start = ((), (), s32[]{:S(2)}) async-start(), calls=%async_computation.4 | async-start | bytes 8912896 | tf_op jit(solution)/shard_map/all_gather | solution.py:12
  146.1 13.5 %copy-start.49 = (f32[6,1024]{1,0:T(8,128)}, f32[6,1024]{1,0:T(8,128)S(1)}, u32[]{:S(2)}) copy-start(f32[6,1024]{1,0:T(8,128)S(1)} %get-tuple-element.80) | copy-start | bytes 73732
  236.8 8.8 %copy-start.57 = (f32[3,1024]{1,0:T(4,128)S(1)}, f32[3,1024]{1,0:T(4,128)}, u32[]{:S(2)}) copy-start(f32[3,1024]{1,0:T(4,128)} %slice.668) | copy-start | bytes 36868
  236.8 8.8 %copy-start.58 = (f32[3,1024]{1,0:T(4,128)S(1)}, f32[3,1024]{1,0:T(4,128)}, u32[]{:S(2)}) copy-start(f32[3,1024]{1,0:T(4,128)} %slice.672) | copy-start | bytes 36868
  236.8 8.8 %copy-start.59 = (f32[3,1024]{1,0:T(4,128)S(1)}, f32[3,1024]{1,0:T(4,128)}, u32[]{:S(2)}) copy-start(f32[3,1024]{1,0:T(4,128)} %slice.667) | copy-start | bytes 36868
  236.8 8.8 %copy-start.60 = (f32[3,1024]{1,0:T(4,128)S(1)}, f32[3,1024]{1,0:T(4,128)}, u32[]{:S(2)}) copy-start(f32[3,1024]{1,0:T(4,128)} %slice.674) | copy-start | bytes 36868
  236.8 8.8 %copy-start.61 = (f32[3,1024]{1,0:T(4,128)S(1)}, f32[3,1024]{1,0:T(4,128)}, u32[]{:S(2)}) copy-start(f32[3,1024]{1,0:T(4,128)} %slice.669) | copy-start | bytes 36868
  236.8 8.8 %copy-start.62 = (f32[3,1024]{1,0:T(4,128)S(1)}, f32[3,1024]{1,0:T(4,128)}, u32[]{:S(2)}) copy-start(f32[3,1024]{1,0:T(4,128)} %slice.675) | copy-start | bytes 36868
  236.8 8.8 %copy-start.63 = (f32[3,1024]{1,0:T(4,128)S(1)}, f32[3,1024]{1,0:T(4,128)}, u32[]{:S(2)}) copy-start(f32[3,1024]{1,0:T(4,128)} %slice.671) | copy-start | bytes 36868
  236.8 8.8 %copy-start.64 = (f32[3,1024]{1,0:T(4,128)S(1)}, f32[3,1024]{1,0:T(4,128)}, u32[]{:S(2)}) copy-start(f32[3,1024]{1,0:T(4,128)} %slice.679) | copy-start | bytes 36868
  236.8 9.6 %copy-start.53 = (f32[2,1024]{1,0:T(2,128)S(1)}, f32[2,1024]{1,0:T(2,128)}, u32[]{:S(2)}) copy-start(f32[2,1024]{1,0:T(2,128)} %slice.666) | copy-start | bytes 24580
  236.9 9.6 %copy-start.55 = (f32[2,1024]{1,0:T(2,128)S(1)}, f32[2,1024]{1,0:T(2,128)}, u32[]{:S(2)}) copy-start(f32[2,1024]{1,0:T(2,128)} %slice.686) | copy-start | bytes 24580
  236.9 9.7 %copy-start.84 = (f32[1,1024]{1,0:T(1,128)S(1)}, f32[1,1024]{1,0:T(1,128)}, u32[]{:S(2)}) copy-start(f32[1,1024]{1,0:T(1,128)} %slice.855) | copy-start | bytes 12292
  236.9 9.7 %copy-start.85 = (f32[1,1024]{1,0:T(1,128)S(1)}, f32[1,1024]{1,0:T(1,128)}, u32[]{:S(2)}) copy-start(f32[1,1024]{1,0:T(1,128)} %slice.864) | copy-start | bytes 12292
  241.3 5.3 %copy-start.43 = (f32[5,1024]{1,0:T(8,128)S(1)}, f32[5,1024]{1,0:T(8,128)}, u32[]{:S(2)}) copy-start(f32[5,1024]{1,0:T(8,128)} %slice.691) | copy-start | bytes 61444
  241.3 5.4 %copy-start.97 = (f32[1,1024]{1,0:T(1,128)S(1)}, f32[1,1024]{1,0:T(1,128)}, u32[]{:S(2)}) copy-start(f32[1,1024]{1,0:T(1,128)} %slice.869) | copy-start | bytes 12292
  241.4 5.5 %copy-start.96 = (f32[1,1024]{1,0:T(1,128)S(1)}, f32[1,1024]{1,0:T(1,128)}, u32[]{:S(2)}) copy-start(f32[1,1024]{1,0:T(1,128)} %slice.854) | copy-start | bytes 12292
  241.4 5.6 %copy-start.37 = (f32[11,1024]{1,0:T(8,128)S(1)}, f32[11,1024]{1,0:T(8,128)}, u32[]{:S(2)}) copy-start(f32[11,1024]{1,0:T(8,128)} %slice.646) | copy-start | bytes 135172
  241.4 5.6 %copy-start.39 = (f32[11,1024]{1,0:T(8,128)S(1)}, f32[11,1024]{1,0:T(8,128)}, u32[]{:S(2)}) copy-start(f32[11,1024]{1,0:T(8,128)} %slice.697) | copy-start | bytes 135172
  243.6 3.4 copy-start.95
  267.8 3.2 copy-start.12
  267.9 3.2 copy-start.77
  271.1 3.3 copy-start.13
  274.4 3.3 copy-start.99
  274.4 3.3 copy-start.100
  274.4 3.4 copy-start.65
  274.5 3.4 copy-start.66
  274.5 4.2 copy-start.98
  274.5 4.3 copy-start.54
  274.5 4.3 copy-start.56
  274.5 4.3 copy-start.68
  274.5 4.3 copy-start.69
  274.5 4.3 copy-start.82
  274.5 4.3 copy-start.83
  274.5 4.4 %copy-start.44 = (f32[5,1024]{1,0:T(8,128)S(1)}, f32[5,1024]{1,0:T(8,128)}, u32[]{:S(2)}) copy-start(f32[5,1024]{1,0:T(8,128)} %slice.691) | copy-start | bytes 61444
  274.5 4.4 %copy-start.50 = (f32[5,1024]{1,0:T(8,128)S(1)}, f32[5,1024]{1,0:T(8,128)}, u32[]{:S(2)}) copy-start(f32[5,1024]{1,0:T(8,128)} %slice.695) | copy-start | bytes 61444
  274.6 4.4 %copy-start.51 = (f32[5,1024]{1,0:T(8,128)S(1)}, f32[5,1024]{1,0:T(8,128)}, u32[]{:S(2)}) copy-start(f32[5,1024]{1,0:T(8,128)} %slice.699) | copy-start | bytes 61444
  274.6 4.5 %copy-start.91 = (f32[1,1024]{1,0:T(1,128)S(1)}, f32[1,1024]{1,0:T(1,128)}, u32[]{:S(2)}) copy-start(f32[1,1024]{1,0:T(1,128)} %slice.826) | copy-start | bytes 12292
  274.6 4.6 %copy-start.90 = (f32[1,1024]{1,0:T(1,128)S(1)}, f32[1,1024]{1,0:T(1,128)}, u32[]{:S(2)}) copy-start(f32[1,1024]{1,0:T(1,128)} %slice.803) | copy-start | bytes 12292
  292.6 3.2 copy-start.17
  292.6 3.2 copy-start.18
  298.5 3.2 copy-start.15
  304.8 3.2 copy-start.19
  304.8 3.2 copy-start.71
  308.1 3.2 copy-start.7
  315.2 16.2 %all-to-all-start = ((f32[16,4,1024]{2,1,0:T(4,128)}), f32[16,4,1024]{2,1,0:T(4,128)S(1)}, u32[]{:S(2)}, u32[]{:S(2)}) async-start(f32[16,4,1024]{2,1,0:T(4,128)} %broadcast_in_dim.48), calls=%async_computation | async-start | bytes 524288 | tf_op jit(solution)/shard_map/all_to_all | solution.py:18
  407.9 25.1 %all-to-all-start.3 = ((bf16[8,384,256]{2,1,0:T(8,128)(2,1)}), bf16[8,384,256]{2,1,0:T(8,128)(2,1)S(1)}, u32[]{:S(2)}, u32[]{:S(2)}) async-start(bf16[8,384,256]{2,1,0:T(8,128)(2,1)} %bitcast.67), calls=%async_computation.3 | async-start | bytes 3145728 | tf_op jit(solution)/shard_map/all_to_all | solution.py:79
  (60 other events, 84.9 us)
Sparse Core Ops, SparseCore 0:
  9.5 74.0 all-gather.1
where the time goes:
time: 448 us; the launch traced here: 441 us
  local copies, waits for them, and re-layouts  254 us (57%)
  other arithmetic  66.5 us (15%)
  blocking collectives  50.8 us (11%)
  waiting for transfers between devices  28.2 us (6%)
  between operations  15.3 us (3%)
  starting transfers between devices  13.2 us (3%)
  matrix products  12.9 us (3%)
    slice x112, local copies, waits for them, and re-layouts, local_states(): lax.associative_scan(chain_link, (decay_re, decay_im, feed_re, feed_im),...  197 us
    all_to_all x2, blocking collectives, sent_to_all(): return lax.all_to_all(copies, axis, split_axis=0, concat_axis=0, tiled=True)  50.8 us
    pad x60, local copies, waits for them, and re-layouts, local_states(): lax.associative_scan(chain_link, (decay_re, decay_im, feed_re, feed_im),...  37.2 us
    all_to_all x1, waiting for transfers between devices, sent_and_summed(): lax.all_to_all(pieces, axis, split_axis=0, concat_axis=0, tiled=True)  20.6 us
    add x1, other arithmetic, local_states(): feed_im = drive_re * proj_im + drive_im * proj_re  14.7 us
    add x30, other arithmetic, local_states(): lax.associative_scan(chain_link, (decay_re, decay_im, feed_re, feed_im),...  12.5 us
    sub x7, other arithmetic, chain_link(): earlier[0] * later[0] - earlier[1] * later[1]  11.8 us
    add x13, other arithmetic, chain_link(): later[0] * earlier[3] + later[1] * earlier[2] + later[3]  10.7 us
  transfers between devices with their start and end apart: 3, of which 2 were waited for; matrix products, arithmetic and copies ran while one was open for 71% of the time, Pallas kernels for 0%

commit v1 on v0

v1 whole, which is shorter than its diff:
```python
import functools
import math

import jax
import jax.numpy as jnp
from jax import lax
from jax.experimental import pallas as pl
from jax.experimental.pallas import tpu as pltpu
from jax.sharding import PartitionSpec as P

rms_eps = 1e-06
f32 = jnp.float32
bf16 = jnp.bfloat16
CHUNKS = 8


def onehot(shape, test):
    row = lax.broadcasted_iota(jnp.int32, shape, 0)
    col = lax.broadcasted_iota(jnp.int32, shape, 1)
    return jnp.where(test(row, col), 1.0, 0.0).astype(bf16)


def split3(x):
    hi = x.astype(bf16)
    rest = x - hi.astype(f32)
    mid = rest.astype(bf16)
    return hi, mid, (rest - mid.astype(f32)).astype(bf16)


def dot(a, b):
    return jnp.dot(a, b, preferred_element_type=f32)


def dot_t(a, b):
    return lax.dot_general(a, b, (((1,), (1,)), ((), ())), preferred_element_type=f32)


def spread_row(x, states):
    groups = x.shape[0]
    width = groups * states
    lanes = onehot((states, width), lambda r, c: r == c % states)
    wide = sum(dot(part, lanes) for part in split3(x))
    row = lax.broadcasted_iota(jnp.int32, wide.shape, 0)
    col = lax.broadcasted_iota(jnp.int32, wide.shape, 1)
    return jnp.sum(jnp.where(row == col // states, wide, 0.0), axis=0, keepdims=True)


def prepare(u_ref, ls_ref, dr_ref, fr_ref, bm_ref, cm_ref, uperm, step_wide, proj_re, proj_im, rows, wout):
    tokens, channels = u_ref.shape
    groups, states = dr_ref.shape
    width = groups * states
    per_group = channels // groups
    span = tokens // CHUNKS
    perm = onehot((tokens, tokens), lambda r, c: c == (r % CHUNKS) * span + r // CHUNKS)
    u_sorted = dot(perm, u_ref[...]).astype(bf16)
    uperm[...] = u_sorted
    decay = spread_row(dr_ref[...], states)
    angular = spread_row(fr_ref[...], states)
    rows[0:1, :] = -decay
    rows[1:2, :] = 0.5 * angular
    modulus = decay * decay + angular * angular
    inv_re = -decay / modulus
    inv_im = -angular / modulus
    step = jnp.exp(ls_ref[...])
    step = sum(dot(perm, part) for part in split3(step))
    group_lanes = onehot((groups, width), lambda r, c: r == c // states)
    step_wide[...] = sum(dot(part, group_lanes) for part in split3(step))
    pick = onehot((channels, per_group), lambda r, c: r % per_group == c)
    row = lax.broadcasted_iota(jnp.int32, (channels, width), 0)
    col = lax.broadcasted_iota(jnp.int32, (channels, width), 1)
    same = row // per_group == col // states
    b_re = dot_t(pick, bm_ref[0].astype(bf16))
    b_im = dot_t(pick, bm_ref[1].astype(bf16))
    w_re = jnp.where(same, b_re * inv_re - b_im * inv_im, 0.0).astype(bf16)
    w_im = jnp.where(same, b_re * inv_im + b_im * inv_re, 0.0).astype(bf16)
    proj_re[...] = dot(u_sorted, w_re)
    proj_im[...] = dot(u_sorted, w_im)
    state_lanes = onehot((states, width), lambda r, c: r == c % states)
    wout[:, :width] = jnp.where(same, dot(cm_ref[0].astype(bf16), state_lanes), 0.0).astype(bf16)
    wout[:, width:] = jnp.where(same, -dot(cm_ref[1].astype(bf16), state_lanes), 0.0).astype(bf16)


SIN = (-1.0 / 6, 1.0 / 120, -1.0 / 5040, 1.0 / 362880, -1.0 / 39916800)
COS = (-0.5, 1.0 / 24, -1.0 / 720, 1.0 / 40320, -1.0 / 3628800)


def series(q, terms):
    total = terms[-1] * q
    for term in terms[-2::-1]:
        total = (total + term) * q
    return total


def first_pass(step_wide, proj_re, proj_im, rows, dec_re, dec_im, ends):
    tokens, width = step_wide.shape
    block = 256

    def one_block(b, _):
        lanes = pl.ds(pl.multiple_of(b * block, block), block)
        minus_decay = jnp.broadcast_to(rows[0:1, lanes], (CHUNKS, block))
        half_angular = jnp.broadcast_to(rows[1:2, lanes], (CHUNKS, block))

        def one_step(i, carry):
            a_re, a_im, x_re, x_im = carry
            at = pl.ds(pl.multiple_of(i * CHUNKS, CHUNKS), CHUNKS)
            step = step_wide[at, lanes]
            half = step * half_angular
            q = half * half
            sine = half + half * series(q, SIN)
            cosine = 1.0 + series(q, COS)
            factor = jnp.exp(step * minus_decay)
            twice = factor * (sine + sine)
            d_re = factor - twice * sine
            d_im = twice * cosine
            less = d_re - 1.0
            p_re = proj_re[at, lanes]
            p_im = proj_im[at, lanes]
            u_re = less * p_re - d_im * p_im
            u_im = less * p_im + d_im * p_re
            dec_re[at, lanes] = d_re
            dec_im[at, lanes] = d_im
            proj_re[at, lanes] = u_re
            proj_im[at, lanes] = u_im
            return (
                d_re * a_re - d_im * a_im,
                d_re * a_im + d_im * a_re,
                d_re * x_re - d_im * x_im + u_re,
                d_re * x_im + d_im * x_re + u_im,
            )

        zero = jnp.zeros((CHUNKS, block), f32)
        found = lax.fori_loop(0, tokens // CHUNKS, one_step, (zero + 1.0, zero, zero, zero), unroll=2)
        for k in range(4):
            ends[k, :, lanes] = found[k]
        return 0

    lax.fori_loop(0, width // block, one_block, 0)


def chain(early, late):
    return (
        early[0] * late[0] - early[1] * late[1],
        early[0] * late[1] + early[1] * late[0],
        late[0] * early[2] - late[1] * early[3] + late[2],
        late[0] * early[3] + late[1] * early[2] + late[3],
    )


def chunk_prefix(ends, total):
    width = ends.shape[2]
    value = tuple(ends[k] for k in range(4))
    row = lax.broadcasted_iota(jnp.int32, value[0].shape, 0)
    unit = (1.0, 0.0, 0.0, 0.0)

    def moved(value, by):
        return tuple(
            jnp.where(row >= by, pltpu.roll(part, by, 0), zero) for part, zero in zip(value, unit)
        )

    for by in (1, 2, 4):
        value = chain(moved(value, by), value)
    for k in range(4):
        for j in range(width // 128):
            total[8 * k + j : 8 * k + j + 1, :] = value[k][CHUNKS - 1 :, 128 * j : 128 * j + 128]
    before = moved(value, 1)
    for k in range(4):
        ends[k] = before[k]


def second_pass(dec_re, dec_im, feed_re, feed_im, ends, carry, states):
    tokens, width = dec_re.shape
    block = 512
    for b in range(width // block):
        lanes = pl.ds(b * block, block)
        lanes_im = pl.ds(width + b * block, block)
        per = block // 128
        h_re = jnp.concatenate([carry[per * b + j : per * b + j + 1, :] for j in range(per)], axis=1)
        h_im = jnp.concatenate([carry[8 + per * b + j : 9 + per * b + j, :] for j in range(per)], axis=1)
        a_re, a_im = ends[0, :, lanes], ends[1, :, lanes]
        x_re = ends[2, :, lanes] + a_re * h_re - a_im * h_im
        x_im = ends[3, :, lanes] + a_re * h_im + a_im * h_re

        def one_step(i, value):
            x_re, x_im = value
            seen = []
            for k in range(2):
                at = pl.ds(pl.multiple_of(i * 2 * CHUNKS + k * CHUNKS, CHUNKS), CHUNKS)
                d_re, d_im = dec_re[at, lanes], dec_im[at, lanes]
                x_re, x_im = (
                    d_re * x_re - d_im * x_im + feed_re[at, lanes],
                    d_re * x_im + d_im * x_re + feed_im[at, lanes],
                )
                seen.append((x_re, x_im))
            both = pl.ds(pl.multiple_of(i * 2 * CHUNKS, 2 * CHUNKS), 2 * CHUNKS)
            states[both, lanes] = jnp.concatenate([seen[0][0], seen[1][0]], axis=0).astype(bf16)
            states[both, lanes_im] = jnp.concatenate([seen[0][1], seen[1][1]], axis=0).astype(bf16)
            return x_re, x_im

        lax.fori_loop(0, tokens // (2 * CHUNKS), one_step, (x_re, x_im), unroll=2)


def read_out(states, wout, uperm, skip_ref):
    tokens = states.shape[0]
    span = tokens // CHUNKS
    out = dot_t(states[...], wout[...]) + skip_ref[...] * uperm[...].astype(f32)
    mixed = jax.nn.gelu(out).astype(bf16)
    back = onehot((tokens, tokens), lambda r, c: r == (c % CHUNKS) * span + c // CHUNKS)
    return dot(back, mixed).astype(bf16)


def first_kernel(u_ref, ls_ref, dr_ref, fr_ref, bm_ref, cm_ref, dec_re, dec_im, feed_re, feed_im, ends, total, uperm, wout, step_wide, rows):
    prepare(u_ref, ls_ref, dr_ref, fr_ref, bm_ref, cm_ref, uperm, step_wide, feed_re, feed_im, rows, wout)
    first_pass(step_wide, feed_re, feed_im, rows, dec_re, dec_im, ends)
    chunk_prefix(ends, total)


def second_kernel(dec_re, dec_im, feed_re, feed_im, ends, uperm, wout, skip_ref, carry, mixed, states):
    second_pass(dec_re, dec_im, feed_re, feed_im, ends, carry, states)
    mixed[...] = read_out(states, wout, uperm, skip_ref)


def gather_pieces(value, axis, dim):
    copies = jnp.broadcast_to(value, (lax.axis_size(axis), *value.shape))
    pieces = lax.all_to_all(copies, axis, split_axis=0, concat_axis=0, tiled=True)
    pieces = jnp.moveaxis(pieces, 0, dim)
    lengths = pieces.shape
    return pieces.reshape(*lengths[:dim], lengths[dim] * lengths[dim + 1], *lengths[dim + 2 :])


def sent_and_summed(value, axis):
    devices = lax.axis_size(axis)
    pieces = jnp.moveaxis(value.reshape(value.shape[0], devices, -1), 1, 0)
    arrived = lax.all_to_all(pieces, axis, split_axis=0, concat_axis=0, tiled=True)
    return arrived.astype(f32).sum(axis=0)


def per_device(
    resid, mixer_in, log_step, decay_real, frequency, input_matrix, output_matrix, skip_gain,
    value_weight, gate_weight, norm_gain, up_weight, down_weight,
):
    both = jnp.concatenate((up_weight, down_weight), axis=1)
    whole = lax.all_gather(both, "sp", axis=0, tiled=True)
    up_whole, down_whole = jnp.split(whole, 2, axis=1)
    tokens, channels = mixer_in.shape
    groups, states = decay_real.shape
    width = groups * states
    wide = jax.ShapeDtypeStruct((tokens, width), f32)
    vmem = pl.BlockSpec(memory_space=pltpu.VMEM)
    dec_re, dec_im, feed_re, feed_im, ends, total, uperm, wout = pl.pallas_call(
        first_kernel,
        out_shape=(
            wide, wide, wide, wide,
            jax.ShapeDtypeStruct((4, CHUNKS, width), f32),
            jax.ShapeDtypeStruct((32, 128), f32),
            jax.ShapeDtypeStruct((tokens, channels), bf16),
            jax.ShapeDtypeStruct((channels, 2 * width), bf16),
        ),
        in_specs=[vmem] * 6,
        out_specs=[vmem] * 8,
        scratch_shapes=[pltpu.VMEM((tokens, width), f32), pltpu.VMEM((8, width), f32)],
        name="ssm_first",
        compiler_params=pltpu.CompilerParams(vmem_limit_bytes=40 * 2**20),
    )(
        mixer_in, log_step, decay_real, frequency,
        input_matrix.reshape(2, width, -1), output_matrix.reshape(2, channels, states),
    )
    everyone = lax.all_gather(total, "sp").reshape(-1, 4, 8, 128)
    here = lax.axis_index("sp")
    h_re = jnp.zeros((8, 128), f32)
    h_im = jnp.zeros((8, 128), f32)
    for j in range(everyone.shape[0]):
        a_re, a_im, x_re, x_im = everyone[j]
        n_re = a_re * h_re - a_im * h_im + x_re
        n_im = a_re * h_im + a_im * h_re + x_im
        h_re = jnp.where(j < here, n_re, h_re)
        h_im = jnp.where(j < here, n_im, h_im)
    carry = jnp.concatenate([h_re, h_im], axis=0)
    mixed_out = pl.pallas_call(
        second_kernel,
        out_shape=jax.ShapeDtypeStruct((tokens, channels), bf16),
        in_specs=[vmem] * 9,
        out_specs=vmem,
        scratch_shapes=[pltpu.VMEM((tokens, 2 * width), bf16)],
        name="ssm_second",
        compiler_params=pltpu.CompilerParams(vmem_limit_bytes=40 * 2**20),
    )(dec_re, dec_im, feed_re, feed_im, ends, uperm, wout, skip_gain.reshape(1, -1), carry)
    channels_all = gather_pieces(mixed_out, "tp", 1)
    value_pre = jnp.dot(channels_all, value_weight, preferred_element_type=f32)
    gate_pre = jnp.dot(channels_all, gate_weight, preferred_element_type=f32)
    updated = (resid.astype(f32) + value_pre * jax.nn.sigmoid(gate_pre)).astype(bf16)
    updated_wide = lax.optimization_barrier(updated).astype(f32)
    whole_rows = gather_pieces(updated, "tp", 1).astype(f32)
    inv_rms = lax.rsqrt(jnp.mean(whole_rows * whole_rows, axis=1, keepdims=True) + rms_eps)
    normed = (whole_rows * inv_rms * norm_gain).astype(bf16)
    raised = jnp.dot(normed, up_whole, preferred_element_type=f32)
    active = jax.nn.relu(raised)
    hidden = (active * active).astype(bf16)
    partials = lax.dot_general(
        hidden, down_whole, (((1,), (1,)), ((), ())), preferred_element_type=f32
    )
    down_sum = sent_and_summed(partials.astype(bf16), "tp")
    return (updated_wide + down_sum).astype(bf16)


def solution(mesh):
    in_specs = (
        P("sp", "tp"), P("sp", "tp"), P("sp", "tp"), P("tp", None), P("tp", None),
        P(None, "tp", None, None), P(None, "tp", None, None), P("tp"),
        P(None, "tp"), P(None, "tp"), P(), P("sp", "tp"), P("sp", "tp"),
    )
    return jax.shard_map(
        per_device, mesh=mesh, in_specs=in_specs, out_specs=P("sp", "tp"), check_vma=False
    )
```

time: 448 us -> 139 us (0.31); the launches traced: 441 us -> 139 us
  local copies, waits for them, and re-layouts: 254 us -> 3.27 us
  other arithmetic: 66.5 us -> 5.16 us
  blocking collectives: 50.8 us -> 75.7 us
  starting transfers between devices: 13.2 us -> 4.56 us
  waiting for transfers between devices: 28.2 us -> 20.6 us
  Pallas kernels: 0 us -> 7.45 us
    slice x137 -> x0, local copies, waits for them, and re-layouts: 198 us -> none  [the longest x112 197 us: local_states(): lax.associative_scan(chain_link, (decay_re, decay_im, feed_re, feed_im),...]
    add x54 -> x0, other arithmetic: 45.5 us -> none  [the longest x1 14.7 us: local_states(): feed_im = drive_re * proj_im + drive_im * proj_re]
    pad x60 -> x0, local copies, waits for them, and re-layouts: 37.2 us -> none  [local_states(): lax.associative_scan(chain_link, (decay_re, decay_im, feed_re, feed_im),...]
    all_gather x0 -> x1, blocking collectives: none -> 22.6 us  [per_device(): everyone = lax.all_gather(total, 'sp').reshape(-1, 4, 8, 128)]
    sub x7 -> x0, other arithmetic: 11.8 us -> none  [chain_link(): earlier[0] * later[0] - earlier[1] * later[1]]
    all_to_all x1 -> x0, starting transfers between devices: 8.63 us -> none  [sent_to_all(): return lax.all_to_all(copies, axis, split_axis=0, concat_axis=0, tiled=True)]
    all_to_all x1 -> x0, waiting for transfers between devices: 7.55 us -> none  [sent_to_all(): return lax.all_to_all(copies, axis, split_axis=0, concat_axis=0, tiled=True)]
    pallas_call x0 -> x2, Pallas kernels: none -> 7.45 us  [the longest x1 5.81 us: per_device(): pl.pallas_call(first_kernel, out_shape=(wide, wide, wide, wide, jax.Shape...]
  transfers between devices with their start and end apart: 3 -> 2, of which waited for: 2 -> 1; matrix products, arithmetic and copies ran while one was open for 71% -> 3% of each run, Pallas kernels for 0% -> 5%
where the time goes in v1:
time: 139 us
  blocking collectives  75.7 us (54%)
  waiting for transfers between devices  20.6 us (15%)
  between operations  13.7 us (10%)
  matrix products  8.59 us (6%)
  Pallas kernels  7.45 us (5%)
  other arithmetic  5.16 us (4%)
  starting transfers between devices  4.56 us (3%)
  local copies, waits for them, and re-layouts  3.27 us (2%)
    all_to_all x2, blocking collectives, gather_pieces(): lax.all_to_all(copies, axis, split_axis=0, concat_axis=0, tiled=True)  53 us
    all_gather x1, blocking collectives, per_device(): everyone = lax.all_gather(total, 'sp').reshape(-1, 4, 8, 128)  22.6 us
    all_to_all x1, waiting for transfers between devices, sent_and_summed(): lax.all_to_all(pieces, axis, split_axis=0, concat_axis=0, tiled=True)  20.6 us
    dot_general x1, matrix products, per_device(): lax.dot_general(hidden, down_whole, (((1,), (1,)), ((), ())), preferred_e...  7.35 us
    pallas_call x1, Pallas kernels, per_device(): pl.pallas_call(first_kernel, out_shape=(wide, wide, wide, wide, jax.Shape...  5.81 us
    all_to_all x1, starting transfers between devices, sent_and_summed(): lax.all_to_all(pieces, axis, split_axis=0, concat_axis=0, tiled=True)  4.52 us
  transfers between devices with their start and end apart: 2, of which 1 were waited for; matrix products, arithmetic and copies ran while one was open for 3% of the time, Pallas kernels for 5%

profile of v1, /device:TPU:1, one launch (start us, length us, event | category | flops | bytes accessed | tf_op | source)
XLA Modules:
  0.0 139.0 jit_solution(3375159240317698407)
XLA Ops:
  6.5 0.0 copy-start
  6.5 0.0 copy-start.7
  6.5 0.0 copy-start.9
  6.5 0.0 copy-start.1
  6.5 0.0 copy-start.2
  6.5 0.0 copy-start.3
  6.6 0.0 copy-start.4
  6.6 0.0 all-gather.3.cloned.1.call-start
  6.6 2.0 %pad_maximum_fusion = bf16[128,2048]{1,0:T(8,128)(2,1)} fusion(bf16[128,1024]{1,0:T(8,128)(2,1)} %param.25, bf16[128,1024]{1,0:T(8,128)(2,1)} %param.24), kind=kLoop, calls=%fused_computation.20 | loop fusion | flops 1048576 | bytes 1048576 | tf_op jit(solution)/shard_map/concatenate | solution.py:241
  8.6 0.0 all-gather.3.cloned.1.call-update
  8.6 0.0 copy-done.7
  8.7 0.3 copy.20
  9.0 0.0 copy-done.9
  9.0 0.0 copy-start.5
  9.0 0.1 copy.21.ls_ref
  9.2 0.0 copy-done.1
  9.2 0.0 copy-done.2
  9.2 0.0 copy-done.3
  9.2 0.0 copy-done.4
  9.2 5.8 %ssm_first.1 = (f32[384,1024]{1,0:T(8,128)S(1)}, f32[384,1024]{1,0:T(8,128)S(1)}, f32[384,1024]{1,0:T(8,128)S(1)}, f32[384,1024]{1,0:T(8,128)S(1)}, f32[4,8,1024...) custom-call(bf16[384,256]{1,0:T(8,128)(2,1)S(1)} %copy-done.2, ...), custom_call_target="tpu_custom_call" | custom-call | tf_op jit(solution)/shard_map/ssm_first/pallas_call | solution.py:249
  15.1 22.6 %all-gather = f32[512,128]{1,0:T(8,128)S(1)} all-gather(f32[32,128]{1,0:T(8,128)S(1)} %get-tuple-element.20), channel_id=2, replica_groups=mesh['sp'=16,'tp'=8] {'sp'}, dimensions={0}, use_global_device_ids=true | all-gather | bytes 278528 | tf_op jit(solution)/shard_map/all_gather | solution.py:267
  37.9 0.0 copy-done.5
  37.9 1.6 %ssm_second.1 = bf16[384,256]{1,0:T(8,128)(2,1)S(1)} custom-call(f32[384,1024]{1,0:T(8,128)S(1)} %get-tuple-element.13.dec_re, f32[384,1024]{1,0:T(8,128)S(1)} %get-tuple-element.14.dec_im, f32[384,1024]{1,0:T(8,128)S(1)} %get-tuple-element.15.feed_re, f32[384,1024]{1,0:T(8,128)S(1)} %get-tuple-element.16.feed_im, f32[4,8,1024]{2,1,0:T(8,128)S(1)} %get-tuple-element.17.ends, ...), custom_call_target="tpu_custom_call" | custom-call | tf_op jit(solution)/shard_map/ssm_second/pallas_call | solution.py:278
  39.5 0.2 copy.22
  39.7 0.1 broadcast_in_dim.8
  39.8 29.1 %all_to_all.15 = bf16[8,384,256]{1,2,0:T(8,128)(2,1)S(1)} all-to-all(bf16[8,384,256]{1,2,0:T(8,128)(2,1)S(1)} %broadcast_in_dim.8), channel_id=1, replica_groups=mesh['sp'=16,'tp'=8] {'tp'}, dimensions={0} | all-to-all | bytes 3145728 | tf_op jit(solution)/shard_map/all_to_all | solution.py:224
  68.9 0.0 copy-done
  68.9 0.0 copy-start.6
  68.9 0.0 copy-start.8
  68.9 0.6 fusion.13
  69.6 0.6 copy-done.6
  70.1 0.0 copy-done.8
  70.2 0.6 fusion.15
  70.8 0.2 copy.23
  71.0 0.1 broadcast_in_dim.9
  71.1 24.0 %all_to_all.16 = bf16[8,384,256]{1,2,0:T(8,128)(2,1)S(1)} all-to-all(bf16[8,384,256]{1,2,0:T(8,128)(2,1)S(1)} %broadcast_in_dim.9), channel_id=1, replica_groups=mesh['sp'=16,'tp'=8] {'tp'}, dimensions={0} | all-to-all | bytes 3145728 | tf_op jit(solution)/shard_map/all_to_all | solution.py:224
  95.1 0.0 copy-start.10
  95.1 0.4 multiply_reduce_fusion
  95.5 0.3 copy-done.10
  95.8 1.6 %fusion.5 = bf16[384,2048]{0,1:T(8,128)(2,1)} fusion(f32[2048]{0:T(1024)S(1)} %copy-done.10, f32[384]{0:T(512)S(1)} %add_rsqrt_fusion, bf16[8,384,256]{1,2,0:T(8,128)(2,1)S(1)} %all_to_all.16), kind=kLoop, calls=%fused_computation.6 | loop fusion | flops 3145728 | bytes 3155456 | tf_op jit(solution)/shard_map/convert_element_type | solution.py:294
  97.4 0.0 all-gather.3.cloned.1.call-done
  97.4 7.3 %fusion.6 = bf16[384,2048]{1,0:T(8,128)(2,1)S(1)} fusion(bf16[2048,2048]{1,0:T(8,128)(2,1)} %all-gather.3.cloned.1.call-done, bf16[384,2048]{0,1:T(8,128)(2,1)} %fusion.5), kind=kOutput, calls=%fused_computation.9 | convolution fusion | flops 3223191552 | bytes 11534336 | tf_op jit(solution)/shard_map/dot_general | solution.py:298
  104.8 1.3 copy.27
  106.1 4.5 %all-to-all-start.2 = ((bf16[8,384,256]{2,1,0:T(8,128)(2,1)}), bf16[8,384,256]{2,1,0:T(8,128)(2,1)S(1)}, u32[]{:S(2)}, u32[]{:S(2)}) async-start(bf16[8,384,256]{2,1,0:T(8,128)(2,1)} %bitcast.434), calls=%async_computation.2 | async-start | bytes 3145728 | tf_op jit(solution)/shard_map/all_to_all | solution.py:233
  110.6 20.6 %all-to-all-done.2 = bf16[8,384,256]{2,1,0:T(8,128)(2,1)S(1)} async-done(((bf16[8,384,256]{2,1,0:T(8,128)(2,1)}), bf16[8,384,256]{2,1,0:T(8,128)(2,1)S(1)}, u32[]{:S(2)}, u32[]{:S(2)}) %all-to-all-start.2) | async-done | bytes 1572896 | tf_op jit(solution)/shard_map/all_to_all | solution.py:233
  131.2 0.2 convert_reduce_fusion
  131.4 0.7 add_convert_fusion
  (11 shorter events, 0.2 us)
Async XLA Ops:
  6.5 62.4 %copy-start = (bf16[2048,256]{1,0:T(8,128)(2,1)S(1)}, bf16[2048,256]{1,0:T(8,128)(2,1)}, u32[]{:S(2)}) copy-start(bf16[2048,256]{1,0:T(8,128)(2,1)} %param.22) | copy-start | bytes 3145732
  6.5 2.1 %copy-start.7 = (f32[2,16,64,16]{2,3,1,0:T(8,128)S(1)}, f32[2,16,64,16]{2,3,1,0:T(8,128)}, u32[]{:S(2)}) copy-start(f32[2,16,64,16]{2,3,1,0:T(8,128)} %param.18) | copy-start | bytes 393220
  6.5 2.5 %copy-start.9 = (f32[384,16]{0,1:T(8,128)S(1)}, f32[384,16]{0,1:T(8,128)}, u32[]{:S(2)}) copy-start(f32[384,16]{0,1:T(8,128)} %param.15) | copy-start | bytes 73732
  6.5 2.7 %copy-start.1 = (f32[2,16,16,64]{3,2,1,0:T(8,128)S(1)}, f32[2,16,16,64]{3,2,1,0:T(8,128)}, u32[]{:S(2)}) copy-start(f32[2,16,16,64]{3,2,1,0:T(8,128)} %param.19) | copy-start | bytes 393220
  6.5 2.7 %copy-start.2 = (bf16[384,256]{1,0:T(8,128)(2,1)S(1)}, bf16[384,256]{1,0:T(8,128)(2,1)}, u32[]{:S(2)}) copy-start(bf16[384,256]{1,0:T(8,128)(2,1)} %u_ref.1) | copy-start | bytes 589828
  6.5 2.7 %copy-start.3 = (f32[16,64]{1,0:T(8,128)S(1)}, f32[16,64]{1,0:T(8,128)}, u32[]{:S(2)}) copy-start(f32[16,64]{1,0:T(8,128)} %dr_ref.1) | copy-start | bytes 12292
  6.6 2.7 %copy-start.4 = (f32[16,64]{1,0:T(8,128)S(1)}, f32[16,64]{1,0:T(8,128)}, u32[]{:S(2)}) copy-start(f32[16,64]{1,0:T(8,128)} %fr_ref.1) | copy-start | bytes 12292
  6.6 90.9 %all-gather.3.cloned.1.call-start = ((), (), s32[]{:S(2)}) async-start(), calls=%async_computation.3 | async-start | bytes 8912896 | tf_op jit(solution)/shard_map/all_gather | solution.py:242
  9.0 28.9 %copy-start.5 = (f32[256]{0:T(256)S(1)}, f32[256]{0:T(256)}, u32[]{:S(2)}) copy-start(f32[256]{0:T(256)} %param.20) | copy-start | bytes 3076
  68.9 1.2 copy-start.6
  68.9 1.2 copy-start.8
  95.1 0.7 copy-start.10
  106.1 25.1 %all-to-all-start.2 = ((bf16[8,384,256]{2,1,0:T(8,128)(2,1)}), bf16[8,384,256]{2,1,0:T(8,128)(2,1)S(1)}, u32[]{:S(2)}, u32[]{:S(2)}) async-start(bf16[8,384,256]{2,1,0:T(8,128)(2,1)} %bitcast.434), calls=%async_computation.2 | async-start | bytes 3145728 | tf_op jit(solution)/shard_map/all_to_all | solution.py:233
Sparse Core Ops, SparseCore 0:
  9.5 74.4 all-gather.2

commit v2 on v1

--- a/solution.py
+++ b/solution.py
@@ -208,98 +208,408 @@
     return dot(back, mixed).astype(bf16)
 
 
-def first_kernel(u_ref, ls_ref, dr_ref, fr_ref, bm_ref, cm_ref, dec_re, dec_im, feed_re, feed_im, ends, total, uperm, wout, step_wide, rows):
+AXES = pl.DeviceIdType.MESH
+SIDE = 4
+
+
+def around(index, by):
+    return lax.rem(index + by + SIDE, SIDE)
+
+
+class Relay:
+    def __init__(self, buf, send_sem, recv_sem, y_first):
+        here = lax.axis_index("sp")
+        z, y = here // SIDE, lax.rem(here, SIDE)
+        self.p, self.q = (y, z) if y_first else (z, y)
+        self.y_first = y_first
+        self.buf, self.send_sem, self.recv_sem = buf, send_sem, recv_sem
+        self.rows = buf.shape[0] // (SIDE * SIDE)
+        self.started = []
+
+    def index(self, dp, dq):
+        p, q = around(self.p, dp), around(self.q, dq)
+        return q * SIDE + p if self.y_first else p * SIDE + q
+
+    def copy(self, number, slot, half, target):
+        rows = self.rows // 2
+        piece = self.buf.at[pl.ds(pl.multiple_of(slot * self.rows + half * rows, rows), rows), :]
+        return pltpu.make_async_remote_copy(
+            src_ref=piece,
+            dst_ref=piece,
+            send_sem=self.send_sem.at[number],
+            recv_sem=self.recv_sem.at[slot * 2 + half],
+            device_id={"sp": target, "tp": lax.axis_index("tp")},
+            device_id_type=AXES,
+        )
+
+    def send(self, slot, half, dp, dq):
+        copy = self.copy(len(self.started), slot, half, self.index(dp, dq))
+        copy.start()
+        self.started.append(copy)
+
+    def arrived(self, dp, dq, half):
+        self.copy(0, self.index(dp, dq), half, self.index(1, 0)).wait_recv()
+
+    def start_p(self):
+        own = self.index(0, 0)
+        for k in range(2):
+            self.send(own, k, 1, 0)
+            self.send(own, 1 - k, -1, 0)
+
+    def send_q(self, slot):
+        for k in range(2):
+            self.send(slot, k, 0, 1)
+            self.send(slot, 1 - k, 0, -1)
+
+    def forward_p(self):
+        self.arrived(-1, 0, 0)
+        self.send(self.index(-1, 0), 0, 1, 0)
+        self.arrived(1, 0, 1)
+        self.send(self.index(1, 0), 1, -1, 0)
+
+    def serve_near(self):
+        self.arrived(-1, 0, 1)
+        self.send_q(self.index(-1, 0))
+        self.arrived(1, 0, 0)
+        self.send_q(self.index(1, 0))
+
+    def serve_far(self):
+        self.arrived(2, 0, 0)
+        self.arrived(2, 0, 1)
+        self.send_q(self.index(2, 0))
+
+    def forward_q(self, dp):
+        self.arrived(dp, -1, 0)
+        self.send(self.index(dp, -1), 0, 0, 1)
+        self.arrived(dp, 1, 1)
+        self.send(self.index(dp, 1), 1, 0, -1)
+
+    def finish(self, dp):
+        self.arrived(dp, -1, 1)
+        self.arrived(dp, 1, 0)
+        self.arrived(dp, 2, 0)
+        self.arrived(dp, 2, 1)
+
+    def drain(self):
+        for copy in self.started:
+            copy.wait_send()
+
+
+class Gather:
+    def __init__(self, buf, send_sem, recv_sem):
+        here = lax.axis_index("tp")
+        self.x, self.core = here // 2, lax.rem(here, 2)
+        self.buf, self.send_sem, self.recv_sem = buf, send_sem, recv_sem
+        self.started = []
+
+    def slot(self, dx, other=False):
+        core = 1 - self.core if other else self.core
+        return around(self.x, dx) * 2 + core
+
+    def copy(self, number, slot, half, target):
+        rows = self.buf.shape[1] // 2
+        piece = self.buf.at[slot, half * rows : half * rows + rows, :]
+        return pltpu.make_async_remote_copy(
+            src_ref=piece,
+            dst_ref=piece,
+            send_sem=self.send_sem.at[number],
+            recv_sem=self.recv_sem.at[slot * 2 + half],
+            device_id={"sp": lax.axis_index("sp"), "tp": target},
+            device_id_type=AXES,
+        )
+
+    def send(self, dx, half, target):
+        copy = self.copy(len(self.started), self.slot(dx), half, target)
+        copy.start()
+        self.started.append(copy)
+
+    def arrived(self, dx, half, other=False):
+        self.copy(0, self.slot(dx, other), half, self.slot(1)).wait_recv()
+
+    def start(self):
+        for k in range(2):
+            self.send(0, k, self.slot(1))
+            self.send(0, 1 - k, self.slot(-1))
+        for k in range(2):
+            self.send(0, k, self.slot(0, True))
+
+    def serve_near(self):
+        self.arrived(-1, 0)
+        self.send(-1, 0, self.slot(1))
+        self.arrived(1, 1)
+        self.send(1, 1, self.slot(-1))
+        self.send(-1, 0, self.slot(0, True))
+        self.send(1, 1, self.slot(0, True))
+        self.arrived(-1, 1)
+        self.send(-1, 1, self.slot(0, True))
+        self.arrived(1, 0)
+        self.send(1, 0, self.slot(0, True))
+
+    def serve_far(self):
+        for k in range(2):
+            self.arrived(2, k)
+            self.send(2, k, self.slot(0, True))
+
+    def finish(self):
+        for dx in (0, -1, 1, 2):
+            for k in range(2):
+                self.arrived(dx, k, True)
+
+    def drain(self):
+        for copy in self.started:
+            copy.wait_send()
+
+
+def layer_kernel(
+    resid_ref, u_ref, ls_ref, dr_ref, fr_ref, bm_ref, cm_ref, skip_ref, vw_ref, gw_ref, gain_ref, up_ref, down_ref,
+    out_ref,
+    up_all, down_all, vg, dec_re, dec_im, feed_re, feed_im, step_wide, rows, ends, total, totals, carry,
+    uperm, wout, states, mixed_all, upd_all, normed, glu, hidden, stage_pair, from_pair, mine,
+    stage_far, stage_right, stage_left, relay_left, relay_right, from_left, from_right,
+    local_sem, up_send, up_recv, down_send, down_recv, tot_send, tot_recv,
+    mix_send, mix_recv, upd_send, upd_recv, pair_send, pair_recv, sum_send, sum_recv,
+):
+    here, lane = lax.axis_index("sp"), lax.axis_index("tp")
+    planes = SIDE * SIDE
+    tokens, piece = resid_ref.shape
+    half = tokens // 2
+    up = Relay(up_all, up_send, up_recv, True)
+    down = Relay(down_all, down_send, down_recv, False)
+    mix = Gather(mixed_all, mix_send, mix_recv)
+    upd = Gather(upd_all, upd_send, upd_recv)
+    right, left, partner = mix.slot(1), mix.slot(-1), mix.slot(0, True)
+
+    barrier = pltpu.get_barrier_semaphore()
+    for by in range(1, planes):
+        pl.semaphore_signal(
+            barrier, inc=1, device_id={"sp": lax.rem(here + by, planes), "tp": lane}, device_id_type=AXES
+        )
+    for target in (right, left, partner):
+        pl.semaphore_signal(barrier, inc=1, device_id={"sp": here, "tp": target}, device_id_type=AXES)
+
+    own_rows = pl.ds(pl.multiple_of(here * up.rows, up.rows), up.rows)
+    local = [
+        pltpu.make_async_copy(up_ref, up_all.at[own_rows, :], local_sem.at[0]),
+        pltpu.make_async_copy(down_ref, down_all.at[own_rows, :], local_sem.at[1]),
+        pltpu.make_async_copy(vw_ref, vg.at[:, :piece], local_sem.at[2]),
+        pltpu.make_async_copy(gw_ref, vg.at[:, piece:], local_sem.at[3]),
+    ]
+    for copy in local:
+        copy.start()
+    local[0].wait()
+    local[1].wait()
+    pl.semaphore_wait(barrier, planes + 2)
+    up.start_p()
+    down.start_p()
+
     prepare(u_ref, ls_ref, dr_ref, fr_ref, bm_ref, cm_ref, uperm, step_wide, feed_re, feed_im, rows, wout)
     first_pass(step_wide, feed_re, feed_im, rows, dec_re, dec_im, ends)
     chunk_prefix(ends, total)
 
-
-def second_kernel(dec_re, dec_im, feed_re, feed_im, ends, uperm, wout, skip_ref, carry, mixed, states):
+    def total_copy(by, slot, target):
+        return pltpu.make_async_remote_copy(
+            src_ref=total,
+            dst_ref=totals.at[slot],
+            send_sem=tot_send.at[by],
+            recv_sem=tot_recv.at[slot],
+            device_id={"sp": target, "tp": lane},
+            device_id_type=AXES,
+        )
+
+    for by in range(1, planes):
+        @pl.when(here + by < planes)
+        def _():
+            total_copy(by, here, lax.rem(here + by, planes)).start()
+
+    up.forward_p()
+    down.forward_p()
+    own_up, own_down = up.index(0, 0), down.index(0, 0)
+    up.send_q(own_up)
+    down.send_q(own_down)
+    up.serve_near()
+    down.serve_near()
+
+    def fold(j, value):
+        h_re, h_im = value
+        total_copy(0, j, lax.rem(here + 1, planes)).wait_recv()
+        a_re, a_im = totals[j, 0:8, :], totals[j, 8:16, :]
+        x_re, x_im = totals[j, 16:24, :], totals[j, 24:32, :]
+        return a_re * h_re - a_im * h_im + x_re, a_re * h_im + a_im * h_re + x_im
+
+    zero = jnp.zeros((8, 128), f32)
+    h_re, h_im = lax.fori_loop(0, here, fold, (zero, zero))
+    carry[0:8, :] = h_re
+    carry[8:16, :] = h_im
     second_pass(dec_re, dec_im, feed_re, feed_im, ends, carry, states)
-    mixed[...] = read_out(states, wout, uperm, skip_ref)
-
-
-def gather_pieces(value, axis, dim):
-    copies = jnp.broadcast_to(value, (lax.axis_size(axis), *value.shape))
-    pieces = lax.all_to_all(copies, axis, split_axis=0, concat_axis=0, tiled=True)
-    pieces = jnp.moveaxis(pieces, 0, dim)
-    lengths = pieces.shape
-    return pieces.reshape(*lengths[:dim], lengths[dim] * lengths[dim + 1], *lengths[dim + 2 :])
-
-
-def sent_and_summed(value, axis):
-    devices = lax.axis_size(axis)
-    pieces = jnp.moveaxis(value.reshape(value.shape[0], devices, -1), 1, 0)
-    arrived = lax.all_to_all(pieces, axis, split_axis=0, concat_axis=0, tiled=True)
-    return arrived.astype(f32).sum(axis=0)
+    mixed_all[lane] = read_out(states, wout, uperm, skip_ref)
+    mix.start()
+    up.serve_far()
+    down.serve_far()
+    mix.serve_near()
+    mix.serve_far()
+    mix.finish()
+
+    local[2].wait()
+    local[3].wait()
+    glu[...] = jnp.zeros_like(glu)
+
+    def glu_step(s, _):
+        at = pl.ds(pl.multiple_of(s * piece, piece), piece)
+        glu[...] += dot(mixed_all[s], vg[at, :])
+        return 0
+
+    slots = mixed_all.shape[0]
+    lax.fori_loop(0, slots, glu_step, 0)
+    updated = (resid_ref[...].astype(f32) + glu[:, :piece] * jax.nn.sigmoid(glu[:, piece:])).astype(bf16)
+    upd_all[lane] = updated
+    upd.start()
+    up.forward_q(0)
+    down.forward_q(0)
+    upd.serve_near()
+    upd.serve_far()
+    up.forward_q(-1)
+    down.forward_q(-1)
+    up.forward_q(1)
+    down.forward_q(1)
+    upd.finish()
+
+    def square_step(s, total):
+        wide = upd_all[s].astype(f32)
+        return total + jnp.sum(wide * wide, axis=1, keepdims=True)
+
+    squares = lax.fori_loop(0, slots, square_step, jnp.zeros((tokens, 1), f32))
+    inv_rms = lax.rsqrt(squares / (slots * piece) + rms_eps)
+    for s in range(slots):
+        at = slice(s * piece, s * piece + piece)
+        normed[:, at] = (upd_all[s].astype(f32) * inv_rms * gain_ref[:, at]).astype(bf16)
+    up.forward_q(2)
+    down.forward_q(2)
+    for dp in (0, -1, 1, 2):
+        up.finish(dp)
+
+    def up_step(n, _):
+        at = pl.ds(pl.multiple_of(n * piece, piece), piece)
+        active = jnp.maximum(dot(normed[...], up_all[:, at]), 0.0)
+        hidden[:, at] = (active * active).astype(bf16)
+        return 0
+
+    lax.fori_loop(0, hidden.shape[1] // piece, up_step, 0)
+    for dp in (0, -1, 1, 2):
+        down.finish(dp)
+
+    def product(slot):
+        at = pl.ds(pl.multiple_of(slot * piece, piece), piece)
+        return dot_t(hidden[...], down_all[at, :])
+
+    def sum_copy(number, src, dst, target, send_sem, recv_sem):
+        return pltpu.make_async_remote_copy(
+            src_ref=src,
+            dst_ref=dst,
+            send_sem=send_sem.at[number],
+            recv_sem=recv_sem.at[number],
+            device_id={"sp": here, "tp": target},
+            device_id_type=AXES,
+        )
+
+    order = (2, 1, -1, 0)
+    pairs = []
+    for k, dx in enumerate(order):
+        stage_pair[k] = product(mix.slot(dx, True)).astype(bf16)
+        copy = sum_copy(k, stage_pair.at[k], from_pair.at[k], partner, pair_send, pair_recv)
+        copy.start()
+        pairs.append(copy)
+    sums = [
+        sum_copy(0, stage_far.at[:half, :], relay_left, right, sum_send, sum_recv),
+        sum_copy(1, stage_far.at[half:, :], relay_right, left, sum_send, sum_recv),
+        sum_copy(2, stage_right.at[half:, :], from_left.at[half:, :], right, sum_send, sum_recv),
+        sum_copy(3, stage_left.at[:half, :], from_right.at[:half, :], left, sum_send, sum_recv),
+        sum_copy(4, stage_right.at[:half, :], from_left.at[:half, :], right, sum_send, sum_recv),
+        sum_copy(5, stage_left.at[half:, :], from_right.at[half:, :], left, sum_send, sum_recv),
+    ]
+    for k, dx in enumerate(order):
+        mine[...] = product(mix.slot(dx))
+        pairs[k].wait_recv()
+        mine[...] += from_pair[k].astype(f32)
+        if k == 0:
+            stage_far[...] = mine[...].astype(bf16)
+            sums[0].start()
+            sums[1].start()
+        elif k == 1:
+            stage_right[half:, :] = mine[half:, :].astype(bf16)
+            sums[2].start()
+            sums[0].wait_recv()
+            stage_right[:half, :] = (mine[:half, :] + relay_left[...].astype(f32)).astype(bf16)
+            sums[4].start()
+        elif k == 2:
+            stage_left[:half, :] = mine[:half, :].astype(bf16)
+            sums[3].start()
+            sums[1].wait_recv()
+            stage_left[half:, :] = (mine[half:, :] + relay_right[...].astype(f32)).astype(bf16)
+            sums[5].start()
+    for k in range(2, 6):
+        sums[k].wait_recv()
+    result = upd_all[lane].astype(f32) + (mine[...] + from_left[...].astype(f32) + from_right[...].astype(f32))
+    out_ref[...] = result.astype(bf16)
+
+    for by in range(1, planes):
+        @pl.when(here + by < planes)
+        def _():
+            total_copy(by, here, lax.rem(here + by, planes)).wait_send()
+
+    for ring in (up, down, mix, upd):
+        ring.drain()
+    for copy in pairs + sums:
+        copy.wait_send()
 
 
 def per_device(
     resid, mixer_in, log_step, decay_real, frequency, input_matrix, output_matrix, skip_gain,
     value_weight, gate_weight, norm_gain, up_weight, down_weight,
 ):
-    both = jnp.concatenate((up_weight, down_weight), axis=1)
-    whole = lax.all_gather(both, "sp", axis=0, tiled=True)
-    up_whole, down_whole = jnp.split(whole, 2, axis=1)
     tokens, channels = mixer_in.shape
     groups, states = decay_real.shape
     width = groups * states
-    wide = jax.ShapeDtypeStruct((tokens, width), f32)
+    planes, slots = lax.axis_size("sp"), lax.axis_size("tp")
+    features = slots * channels
+    hidden = up_weight.shape[1]
     vmem = pl.BlockSpec(memory_space=pltpu.VMEM)
-    dec_re, dec_im, feed_re, feed_im, ends, total, uperm, wout = pl.pallas_call(
-        first_kernel,
-        out_shape=(
-            wide, wide, wide, wide,
-            jax.ShapeDtypeStruct((4, CHUNKS, width), f32),
-            jax.ShapeDtypeStruct((32, 128), f32),
-            jax.ShapeDtypeStruct((tokens, channels), bf16),
-            jax.ShapeDtypeStruct((channels, 2 * width), bf16),
+    hbm = pl.BlockSpec(memory_space=pl.ANY)
+    wide = pltpu.VMEM((tokens, width), f32)
+    block = pltpu.VMEM((tokens, channels), bf16)
+    halves = pltpu.VMEM((tokens // 2, channels), bf16)
+    dma = pltpu.SemaphoreType.DMA
+    return pl.pallas_call(
+        layer_kernel,
+        out_shape=jax.ShapeDtypeStruct((tokens, channels), bf16),
+        in_specs=[vmem] * 8 + [hbm] * 2 + [vmem] + [hbm] * 2,
+        out_specs=vmem,
+        scratch_shapes=[
+            pltpu.VMEM((features, hidden), bf16), pltpu.VMEM((features, hidden), bf16),
+            pltpu.VMEM((features, 2 * channels), bf16),
+            wide, wide, wide, wide, wide,
+            pltpu.VMEM((8, width), f32), pltpu.VMEM((4, CHUNKS, width), f32),
+            pltpu.VMEM((32, 128), f32), pltpu.VMEM((planes, 32, 128), f32), pltpu.VMEM((16, 128), f32),
+            block, pltpu.VMEM((channels, 2 * width), bf16), pltpu.VMEM((tokens, 2 * width), bf16),
+            pltpu.VMEM((slots, tokens, channels), bf16), pltpu.VMEM((slots, tokens, channels), bf16),
+            pltpu.VMEM((tokens, features), bf16), pltpu.VMEM((tokens, 2 * channels), f32),
+            pltpu.VMEM((tokens, hidden), bf16),
+            pltpu.VMEM((4, tokens, channels), bf16), pltpu.VMEM((4, tokens, channels), bf16),
+            pltpu.VMEM((tokens, channels), f32),
+            block, block, block, halves, halves, block, block,
+            dma((4,)), dma((30,)), dma((2 * planes,)), dma((30,)), dma((2 * planes,)),
+            dma((planes,)), dma((planes,)),
+            dma((14,)), dma((2 * slots,)), dma((14,)), dma((2 * slots,)),
+            dma((4,)), dma((4,)), dma((6,)), dma((6,)),
+        ],
+        name="layer",
+        compiler_params=pltpu.CompilerParams(
+            vmem_limit_bytes=58 * 2**20, collective_id=0, has_side_effects=True
         ),
-        in_specs=[vmem] * 6,
-        out_specs=[vmem] * 8,
-        scratch_shapes=[pltpu.VMEM((tokens, width), f32), pltpu.VMEM((8, width), f32)],
-        name="ssm_first",
-        compiler_params=pltpu.CompilerParams(vmem_limit_bytes=40 * 2**20),
     )(
-        mixer_in, log_step, decay_real, frequency,
+        resid, mixer_in, log_step, decay_real, frequency,
         input_matrix.reshape(2, width, -1), output_matrix.reshape(2, channels, states),
+        skip_gain.reshape(1, -1), value_weight, gate_weight, norm_gain.reshape(1, -1), up_weight, down_weight,
     )
-    everyone = lax.all_gather(total, "sp").reshape(-1, 4, 8, 128)
-    here = lax.axis_index("sp")
-    h_re = jnp.zeros((8, 128), f32)
-    h_im = jnp.zeros((8, 128), f32)
-    for j in range(everyone.shape[0]):
-        a_re, a_im, x_re, x_im = everyone[j]
-        n_re = a_re * h_re - a_im * h_im + x_re
-        n_im = a_re * h_im + a_im * h_re + x_im
-        h_re = jnp.where(j < here, n_re, h_re)
-        h_im = jnp.where(j < here, n_im, h_im)
-    carry = jnp.concatenate([h_re, h_im], axis=0)
-    mixed_out = pl.pallas_call(
-        second_kernel,
-        out_shape=jax.ShapeDtypeStruct((tokens, channels), bf16),
-        in_specs=[vmem] * 9,
-        out_specs=vmem,
-        scratch_shapes=[pltpu.VMEM((tokens, 2 * width), bf16)],
-        name="ssm_second",
-        compiler_params=pltpu.CompilerParams(vmem_limit_bytes=40 * 2**20),
-    )(dec_re, dec_im, feed_re, feed_im, ends, uperm, wout, skip_gain.reshape(1, -1), carry)
-    channels_all = gather_pieces(mixed_out, "tp", 1)
-    value_pre = jnp.dot(channels_all, value_weight, preferred_element_type=f32)
-    gate_pre = jnp.dot(channels_all, gate_weight, preferred_element_type=f32)
-    updated = (resid.astype(f32) + value_pre * jax.nn.sigmoid(gate_pre)).astype(bf16)
-    updated_wide = lax.optimization_barrier(updated).astype(f32)
-    whole_rows = gather_pieces(updated, "tp", 1).astype(f32)
-    inv_rms = lax.rsqrt(jnp.mean(whole_rows * whole_rows, axis=1, keepdims=True) + rms_eps)
-    normed = (whole_rows * inv_rms * norm_gain).astype(bf16)
-    raised = jnp.dot(normed, up_whole, preferred_element_type=f32)
-    active = jax.nn.relu(raised)
-    hidden = (active * active).astype(bf16)
-    partials = lax.dot_general(
-        hidden, down_whole, (((1,), (1,)), ((), ())), preferred_element_type=f32
-    )
-    down_sum = sent_and_summed(partials.astype(bf16), "tp")
-    return (updated_wide + down_sum).astype(bf16)
 
 
 def solution(mesh):

time: 139 us -> 80.6 us (0.58)
  blocking collectives: 75.7 us -> 0 us
  Pallas kernels: 7.45 us -> 73.9 us
  waiting for transfers between devices: 20.6 us -> 0 us
  between operations: 13.7 us -> 0.01 us
  matrix products: 8.59 us -> 0 us
  other arithmetic: 5.16 us -> 0 us
  starting transfers between devices: 4.56 us -> 0 us
  local copies, waits for them, and re-layouts: 3.27 us -> 5.46 us
    pallas_call x2 -> x1, Pallas kernels: 7.45 us -> 73.9 us  [per_device(): pl.pallas_call(layer_kernel, out_shape=jax.ShapeDtypeStruct((tokens, chan...]
    all_to_all x2 -> x0, blocking collectives: 53 us -> none  [gather_pieces(): lax.all_to_all(copies, axis, split_axis=0, concat_axis=0, tiled=True)]
    all_gather x1 -> x0, blocking collectives: 22.6 us -> none  [per_device(): everyone = lax.all_gather(total, 'sp').reshape(-1, 4, 8, 128)]
    all_to_all x1 -> x0, waiting for transfers between devices: 20.6 us -> none  [sent_and_summed(): lax.all_to_all(pieces, axis, split_axis=0, concat_axis=0, tiled=True)]
    dot_general x3 -> x0, matrix products: 8.59 us -> none  [the longest x1 7.35 us: per_device(): lax.dot_general(hidden, down_whole, (((1,), (1,)), ((), ())), preferred_e...]
    all_to_all x1 -> x0, starting transfers between devices: 4.52 us -> none  [sent_and_summed(): lax.all_to_all(pieces, axis, split_axis=0, concat_axis=0, tiled=True)]
    unnamed x24 -> x3, local copies, waits for them, and re-layouts: 1.38 us -> 5.46 us
    convert_element_type x2 -> x0, other arithmetic: 2.38 us -> none  [the longest x1 1.65 us: per_device(): normed = (whole_rows * inv_rms * norm_gain).astype(bf16)]
  transfers between devices with their start and end apart: 2 -> 0, of which waited for: 1 -> 0; matrix products, arithmetic and copies ran while one was open for 3% -> 0% of each run, Pallas kernels for 5% -> 0%
where the time goes in v2:
time: 80.6 us; the launch traced here: 79.4 us
  Pallas kernels  73.9 us (92%)
  local copies, waits for them, and re-layouts  5.46 us (7%)
    pallas_call x1, Pallas kernels, per_device(): pl.pallas_call(layer_kernel, out_shape=jax.ShapeDtypeStruct((tokens, chan...  73.9 us
    unnamed x3, local copies, waits for them, and re-layouts  5.46 us

profile of v2, /device:TPU:1, one launch (start us, length us, event | category | flops | bytes accessed | tf_op | source)
XLA Modules:
  0.0 79.4 jit_solution(7100911406155034242)
XLA Ops:
  0.0 1.5 %copy.15.ls_ref = f32[384,16]{1,0:T(8,128)} copy(f32[384,16]{0,1:T(8,128)} %param.15) | data formatting | bytes 49152 | tf_op args[2]
  1.5 2.3 %copy.14 = f32[2,16,64,16]{3,2,1,0:T(8,128)} copy(f32[2,16,64,16]{2,3,1,0:T(8,128)} %param.18) | data formatting | bytes 262144 | tf_op args[5]
  3.8 73.9 %layer.1 = bf16[384,256]{1,0:T(8,128)(2,1)} custom-call(bf16[384,256]{1,0:T(8,128)(2,1)} %resid_ref.1, bf16[384,256]{1,0:T(8,128)(2,1)} %u_ref.1, f32[384,16]{1,0:T(8,128)} %copy.15.ls_ref, f32[16,64]{1,0:T(8,128)} %dr_ref.1, f32[16,64]{1,0:T(8,128)} %fr_ref.1, f32[2,1024,16]{2,1,0:T(8,128)} %bitcast.4, f32[2,256,64]{2,1,0:T(8,128)} %bitcast.5, ...), custom_call_target="tpu_custom_call" | custom-call | tf_op jit(solution)/shard_map/layer/pallas_call | solution.py:581
  77.8 1.6 %copy.17 = bf16[384,256]{1,0:T(8,128)(2,1)} copy(bf16[384,256]{1,0:T(8,128)(2,1)} %layer.1) | data formatting | bytes 393216

commit v3 on v2

--- a/solution.py
+++ b/solution.py
@@ -62,20 +62,19 @@
     inv_re = -decay / modulus
     inv_im = -angular / modulus
     step = jnp.exp(ls_ref[...])
-    step = sum(dot(perm, part) for part in split3(step))
+    step = sum(dot_t(perm, part) for part in split3(step))
     group_lanes = onehot((groups, width), lambda r, c: r == c // states)
     step_wide[...] = sum(dot(part, group_lanes) for part in split3(step))
-    pick = onehot((channels, per_group), lambda r, c: r % per_group == c)
+    state_lanes = onehot((states, width), lambda r, c: r == c % states)
     row = lax.broadcasted_iota(jnp.int32, (channels, width), 0)
     col = lax.broadcasted_iota(jnp.int32, (channels, width), 1)
     same = row // per_group == col // states
-    b_re = dot_t(pick, bm_ref[0].astype(bf16))
-    b_im = dot_t(pick, bm_ref[1].astype(bf16))
+    b_re = dot(bm_ref[0].astype(bf16), state_lanes)
+    b_im = dot(bm_ref[1].astype(bf16), state_lanes)
     w_re = jnp.where(same, b_re * inv_re - b_im * inv_im, 0.0).astype(bf16)
     w_im = jnp.where(same, b_re * inv_im + b_im * inv_re, 0.0).astype(bf16)
     proj_re[...] = dot(u_sorted, w_re)
     proj_im[...] = dot(u_sorted, w_im)
-    state_lanes = onehot((states, width), lambda r, c: r == c % states)
     wout[:, :width] = jnp.where(same, dot(cm_ref[0].astype(bf16), state_lanes), 0.0).astype(bf16)
     wout[:, width:] = jnp.where(same, -dot(cm_ref[1].astype(bf16), state_lanes), 0.0).astype(bf16)
 
@@ -91,7 +90,7 @@
     return total
 
 
-def first_pass(step_wide, proj_re, proj_im, rows, dec_re, dec_im, ends):
+def first_pass(step_wide, proj_re, proj_im, rows, dec_re, dec_im, ends, first, last):
     tokens, width = step_wide.shape
     block = 256
 
@@ -134,7 +133,7 @@
             ends[k, :, lanes] = found[k]
         return 0
 
-    lax.fori_loop(0, width // block, one_block, 0)
+    lax.fori_loop(first, last, one_block, 0)
 
 
 def chain(early, late):
@@ -256,8 +255,8 @@
             self.send(own, k, 1, 0)
             self.send(own, 1 - k, -1, 0)
 
-    def send_q(self, slot):
-        for k in range(2):
+    def send_q(self, slot, part=(0, 1)):
+        for k in part:
             self.send(slot, k, 0, 1)
             self.send(slot, 1 - k, 0, -1)
 
@@ -284,11 +283,13 @@
         self.arrived(dp, 1, 1)
         self.send(self.index(dp, 1), 1, 0, -1)
 
-    def finish(self, dp):
-        self.arrived(dp, -1, 1)
-        self.arrived(dp, 1, 0)
-        self.arrived(dp, 2, 0)
-        self.arrived(dp, 2, 1)
+    def finish(self, dq):
+        for dp in (0, -1, 1, 2):
+            if dq == 2:
+                self.arrived(dp, 2, 0)
+                self.arrived(dp, 2, 1)
+            elif dq:
+                self.arrived(dp, dq, 1 if dq == -1 else 0)
 
     def drain(self):
         for copy in self.started:
@@ -360,15 +361,29 @@
             copy.wait_send()
 
 
+class Phases:
+    def __init__(self):
+        self.scope = None
+
+    def __call__(self, name):
+        if self.scope is not None:
+            self.scope.__exit__(None, None, None)
+        self.scope = jax.named_scope(name) if name else None
+        if self.scope is not None:
+            self.scope.__enter__()
+
+
 def layer_kernel(
-    resid_ref, u_ref, ls_ref, dr_ref, fr_ref, bm_ref, cm_ref, skip_ref, vw_ref, gw_ref, gain_ref, up_ref, down_ref,
+    resid_hbm, u_hbm, ls_hbm, dr_hbm, fr_hbm, bm_hbm, cm_hbm, skip_hbm, gain_hbm, vw_ref, gw_ref, up_ref, down_ref,
     out_ref,
+    resid_ref, u_ref, ls_ref, dr_ref, fr_ref, bm_ref, cm_ref, skip_ref, gain_ref,
     up_all, down_all, vg, dec_re, dec_im, feed_re, feed_im, step_wide, rows, ends, total, totals, carry,
-    uperm, wout, states, mixed_all, upd_all, normed, glu, hidden, stage_pair, from_pair, mine,
+    uperm, wout, states, mixed_all, upd_all, normed, glu, raised, hidden, stage_pair, from_pair, mine,
     stage_far, stage_right, stage_left, relay_left, relay_right, from_left, from_right,
-    local_sem, up_send, up_recv, down_send, down_recv, tot_send, tot_recv,
+    local_sem, round_sem, up_send, up_recv, down_send, down_recv, tot_send, tot_recv,
     mix_send, mix_recv, upd_send, upd_recv, pair_send, pair_recv, sum_send, sum_recv,
 ):
+    phase = Phases()
     here, lane = lax.axis_index("sp"), lax.axis_index("tp")
     planes = SIDE * SIDE
     tokens, piece = resid_ref.shape
@@ -378,33 +393,58 @@
     mix = Gather(mixed_all, mix_send, mix_recv)
     upd = Gather(upd_all, upd_send, upd_recv)
     right, left, partner = mix.slot(1), mix.slot(-1), mix.slot(0, True)
-
+    near_planes = [up.index(*by) for by in ((1, 0), (-1, 0), (0, 1), (0, -1))]
+
+    phase("signal")
     barrier = pltpu.get_barrier_semaphore()
-    for by in range(1, planes):
-        pl.semaphore_signal(
-            barrier, inc=1, device_id={"sp": lax.rem(here + by, planes), "tp": lane}, device_id_type=AXES
-        )
+    for target in near_planes:
+        pl.semaphore_signal(barrier, inc=1, device_id={"sp": target, "tp": lane}, device_id_type=AXES)
     for target in (right, left, partner):
         pl.semaphore_signal(barrier, inc=1, device_id={"sp": here, "tp": target}, device_id_type=AXES)
 
     own_rows = pl.ds(pl.multiple_of(here * up.rows, up.rows), up.rows)
-    local = [
-        pltpu.make_async_copy(up_ref, up_all.at[own_rows, :], local_sem.at[0]),
-        pltpu.make_async_copy(down_ref, down_all.at[own_rows, :], local_sem.at[1]),
-        pltpu.make_async_copy(vw_ref, vg.at[:, :piece], local_sem.at[2]),
-        pltpu.make_async_copy(gw_ref, vg.at[:, piece:], local_sem.at[3]),
-    ]
+    moves = (
+        (up_ref, up_all.at[own_rows, :]), (down_ref, down_all.at[own_rows, :]),
+        (u_hbm, u_ref), (dr_hbm, dr_ref), (fr_hbm, fr_ref), (ls_hbm, ls_ref), (bm_hbm, bm_ref), (cm_hbm, cm_ref),
+        (skip_hbm, skip_ref), (vw_ref, vg.at[:, :piece]), (gw_ref, vg.at[:, piece:]),
+        (resid_hbm, resid_ref), (gain_hbm, gain_ref),
+    )
+    local = [pltpu.make_async_copy(src, dst, local_sem.at[k]) for k, (src, dst) in enumerate(moves)]
     for copy in local:
         copy.start()
     local[0].wait()
     local[1].wait()
-    pl.semaphore_wait(barrier, planes + 2)
+    phase("barrier")
+    pl.semaphore_wait(barrier, 7)
+    phase("start_p")
+    own_up, own_down = up.index(0, 0), down.index(0, 0)
     up.start_p()
     down.start_p()
-
+    up.send_q(own_up, (0,))
+    down.send_q(own_down, (0,))
+
+    def greet(number):
+        for target in near_planes:
+            pl.semaphore_signal(
+                round_sem.at[number], inc=1, device_id={"sp": target, "tp": lane}, device_id_type=AXES
+            )
+
+    greet(0)
+    for copy in local[2:8]:
+        copy.wait()
+    phase("prepare")
     prepare(u_ref, ls_ref, dr_ref, fr_ref, bm_ref, cm_ref, uperm, step_wide, feed_re, feed_im, rows, wout)
-    first_pass(step_wide, feed_re, feed_im, rows, dec_re, dec_im, ends)
+    pl.semaphore_wait(round_sem.at[0], 4)
+    greet(1)
+    phase("first_pass")
+    scan_refs = (step_wide, feed_re, feed_im, rows, dec_re, dec_im, ends)
+    first_pass(*scan_refs, 0, 2)
+    pl.semaphore_wait(round_sem.at[1], 4)
+    greet(2)
+    first_pass(*scan_refs, 2, 4)
+    phase("chunk")
     chunk_prefix(ends, total)
+    pl.semaphore_wait(round_sem.at[2], 4)
 
     def total_copy(by, slot, target):
         return pltpu.make_async_remote_copy(
@@ -416,18 +456,23 @@
             device_id_type=AXES,
         )
 
+    phase("totals")
     for by in range(1, planes):
         @pl.when(here + by < planes)
         def _():
             total_copy(by, here, lax.rem(here + by, planes)).start()
 
+    phase("forward_p")
     up.forward_p()
     down.forward_p()
-    own_up, own_down = up.index(0, 0), down.index(0, 0)
-    up.send_q(own_up)
-    down.send_q(own_down)
+    phase("send_q")
+    up.send_q(own_up, (1,))
+    down.send_q(own_down, (1,))
+    phase("serve_near")
     up.serve_near()
     down.serve_near()
+
+    phase("fold")
 
     def fold(j, value):
         h_re, h_im = value
@@ -440,17 +485,31 @@
     h_re, h_im = lax.fori_loop(0, here, fold, (zero, zero))
     carry[0:8, :] = h_re
     carry[8:16, :] = h_im
+    phase("second_pass")
     second_pass(dec_re, dec_im, feed_re, feed_im, ends, carry, states)
+    local[8].wait()
+    phase("read_out")
     mixed_all[lane] = read_out(states, wout, uperm, skip_ref)
+    phase("mix_start")
     mix.start()
+    phase("serve_far")
     up.serve_far()
     down.serve_far()
+    up.forward_q(0)
+    down.forward_q(0)
+    phase("mix_near")
     mix.serve_near()
+    phase("mix_far")
     mix.serve_far()
+    phase("fq_minus")
+    up.forward_q(-1)
+    down.forward_q(-1)
+    phase("mix_finish")
     mix.finish()
 
-    local[2].wait()
-    local[3].wait()
+    phase("glu")
+    for copy in local[9:]:
+        copy.wait()
     glu[...] = jnp.zeros_like(glu)
 
     def glu_step(s, _):
@@ -462,16 +521,22 @@
     lax.fori_loop(0, slots, glu_step, 0)
     updated = (resid_ref[...].astype(f32) + glu[:, :piece] * jax.nn.sigmoid(glu[:, piece:])).astype(bf16)
     upd_all[lane] = updated
+    phase("upd_start")
     upd.start()
-    up.forward_q(0)
-    down.forward_q(0)
-    upd.serve_near()
-    upd.serve_far()
-    up.forward_q(-1)
-    down.forward_q(-1)
+    phase("fq_plus")
     up.forward_q(1)
     down.forward_q(1)
+    phase("upd_near")
+    upd.serve_near()
+    phase("fq_far")
+    up.forward_q(2)
+    down.forward_q(2)
+    phase("upd_far")
+    upd.serve_far()
+    phase("upd_finish")
     upd.finish()
+
+    phase("norm")
 
     def square_step(s, total):
         wide = upd_all[s].astype(f32)
@@ -481,21 +546,35 @@
     inv_rms = lax.rsqrt(squares / (slots * piece) + rms_eps)
     for s in range(slots):
         at = slice(s * piece, s * piece + piece)
-        normed[:, at] = (upd_all[s].astype(f32) * inv_rms * gain_ref[:, at]).astype(bf16)
-    up.forward_q(2)
-    down.forward_q(2)
-    for dp in (0, -1, 1, 2):
-        up.finish(dp)
-
-    def up_step(n, _):
-        at = pl.ds(pl.multiple_of(n * piece, piece), piece)
-        active = jnp.maximum(dot(normed[...], up_all[:, at]), 0.0)
-        hidden[:, at] = (active * active).astype(bf16)
-        return 0
-
-    lax.fori_loop(0, hidden.shape[1] // piece, up_step, 0)
-    for dp in (0, -1, 1, 2):
-        down.finish(dp)
+        normed[s // 2, :, s % 2 * piece : s % 2 * piece + piece] = (
+            upd_all[s].astype(f32) * inv_rms * gain_ref[:, at]
+        ).astype(bf16)
+
+    width = hidden.shape[1]
+    depth = normed.shape[2]
+    for k, dq in enumerate((0, -1, 1, 2)):
+        phase(f"up_wait{k}")
+        up.finish(dq)
+        phase(f"up_mm{k}")
+        group = around(up.q, dq)
+        deep = pl.ds(pl.multiple_of(group * depth, depth), depth)
+
+        def up_step(n, _):
+            at = pl.ds(pl.multiple_of(n * piece, piece), piece)
+            product = dot(normed[group], up_all[deep, at])
+            if k:
+                product = product + raised[:, at]
+            if k < 3:
+                raised[:, at] = product
+            else:
+                active = jnp.maximum(product, 0.0)
+                hidden[:, at] = (active * active).astype(bf16)
+            return 0
+
+        lax.fori_loop(0, width // piece, up_step, 0)
+    phase("down_finish")
+    for dq in (0, -1, 1, 2):
+        down.finish(dq)
 
     def product(slot):
         at = pl.ds(pl.multiple_of(slot * piece, piece), piece)
@@ -512,12 +591,9 @@
         )
 
     order = (2, 1, -1, 0)
-    pairs = []
-    for k, dx in enumerate(order):
-        stage_pair[k] = product(mix.slot(dx, True)).astype(bf16)
-        copy = sum_copy(k, stage_pair.at[k], from_pair.at[k], partner, pair_send, pair_recv)
-        copy.start()
-        pairs.append(copy)
+    pairs = [
+        sum_copy(k, stage_pair.at[k], from_pair.at[k], partner, pair_send, pair_recv) for k in range(len(order))
+    ]
     sums = [
         sum_copy(0, stage_far.at[:half, :], relay_left, right, sum_send, sum_recv),
         sum_copy(1, stage_far.at[half:, :], relay_right, left, sum_send, sum_recv),
@@ -526,31 +602,54 @@
         sum_copy(4, stage_right.at[:half, :], from_left.at[:half, :], right, sum_send, sum_recv),
         sum_copy(5, stage_left.at[half:, :], from_right.at[half:, :], left, sum_send, sum_recv),
     ]
-    for k, dx in enumerate(order):
-        mine[...] = product(mix.slot(dx))
+
+    def pair_step(k):
+        stage_pair[k] = product(mix.slot(order[k], True)).astype(bf16)
+        pairs[k].start()
+
+    def own_step(k):
+        mine[k] = product(mix.slot(order[k]))
+
+    def pair_sum(k):
         pairs[k].wait_recv()
-        mine[...] += from_pair[k].astype(f32)
-        if k == 0:
-            stage_far[...] = mine[...].astype(bf16)
-            sums[0].start()
-            sums[1].start()
-        elif k == 1:
-            stage_right[half:, :] = mine[half:, :].astype(bf16)
-            sums[2].start()
-            sums[0].wait_recv()
-            stage_right[:half, :] = (mine[:half, :] + relay_left[...].astype(f32)).astype(bf16)
-            sums[4].start()
-        elif k == 2:
-            stage_left[:half, :] = mine[:half, :].astype(bf16)
-            sums[3].start()
-            sums[1].wait_recv()
-            stage_left[half:, :] = (mine[half:, :] + relay_right[...].astype(f32)).astype(bf16)
-            sums[5].start()
+        return mine[k] + from_pair[k].astype(f32)
+
+    phase("products")
+    pair_step(0)
+    own_step(0)
+    pair_step(1)
+    pair_step(2)
+    phase("far")
+    stage_far[...] = pair_sum(0).astype(bf16)
+    sums[0].start()
+    sums[1].start()
+    phase("near")
+    own_step(1)
+    own_step(2)
+    mine[1] = pair_sum(1)
+    stage_right[half:, :] = mine[1, half:, :].astype(bf16)
+    sums[2].start()
+    mine[2] = pair_sum(2)
+    stage_left[:half, :] = mine[2, :half, :].astype(bf16)
+    sums[3].start()
+    pair_step(3)
+    own_step(3)
+    phase("relay")
+    sums[0].wait_recv()
+    stage_right[:half, :] = (mine[1, :half, :] + relay_left[...].astype(f32)).astype(bf16)
+    sums[4].start()
+    sums[1].wait_recv()
+    stage_left[half:, :] = (mine[2, half:, :] + relay_right[...].astype(f32)).astype(bf16)
+    sums[5].start()
+    mine[3] = pair_sum(3) + upd_all[lane].astype(f32)
+    phase("sum_wait")
     for k in range(2, 6):
         sums[k].wait_recv()
-    result = upd_all[lane].astype(f32) + (mine[...] + from_left[...].astype(f32) + from_right[...].astype(f32))
+    phase("result")
+    result = mine[3] + (from_left[...].astype(f32) + from_right[...].astype(f32))
     out_ref[...] = result.astype(bf16)
 
+    phase("drain")
     for by in range(1, planes):
         @pl.when(here + by < planes)
         def _():
@@ -560,6 +659,7 @@
         ring.drain()
     for copy in pairs + sums:
         copy.wait_send()
+    phase(None)
 
 
 def per_device(
@@ -581,9 +681,13 @@
     return pl.pallas_call(
         layer_kernel,
         out_shape=jax.ShapeDtypeStruct((tokens, channels), bf16),
-        in_specs=[vmem] * 8 + [hbm] * 2 + [vmem] + [hbm] * 2,
+        in_specs=[hbm] * 13,
         out_specs=vmem,
         scratch_shapes=[
+            block, block, pltpu.VMEM((groups, tokens), f32),
+            pltpu.VMEM((groups, states), f32), pltpu.VMEM((groups, states), f32),
+            pltpu.VMEM((2, channels, states), f32), pltpu.VMEM((2, channels, states), f32),
+            pltpu.VMEM((1, channels), f32), pltpu.VMEM((1, features), f32),
             pltpu.VMEM((features, hidden), bf16), pltpu.VMEM((features, hidden), bf16),
             pltpu.VMEM((features, 2 * channels), bf16),
             wide, wide, wide, wide, wide,
@@ -591,12 +695,12 @@
             pltpu.VMEM((32, 128), f32), pltpu.VMEM((planes, 32, 128), f32), pltpu.VMEM((16, 128), f32),
             block, pltpu.VMEM((channels, 2 * width), bf16), pltpu.VMEM((tokens, 2 * width), bf16),
             pltpu.VMEM((slots, tokens, channels), bf16), pltpu.VMEM((slots, tokens, channels), bf16),
-            pltpu.VMEM((tokens, features), bf16), pltpu.VMEM((tokens, 2 * channels), f32),
-            pltpu.VMEM((tokens, hidden), bf16),
+            pltpu.VMEM((SIDE, tokens, features // SIDE), bf16), pltpu.VMEM((tokens, 2 * channels), f32),
+            pltpu.VMEM((tokens, hidden), f32), pltpu.VMEM((tokens, hidden), bf16),
             pltpu.VMEM((4, tokens, channels), bf16), pltpu.VMEM((4, tokens, channels), bf16),
-            pltpu.VMEM((tokens, channels), f32),
+            pltpu.VMEM((4, tokens, channels), f32),
             block, block, block, halves, halves, block, block,
-            dma((4,)), dma((30,)), dma((2 * planes,)), dma((30,)), dma((2 * planes,)),
+            dma((13,)), pltpu.SemaphoreType.REGULAR((3,)), dma((30,)), dma((2 * planes,)), dma((30,)), dma((2 * planes,)),
             dma((planes,)), dma((planes,)),
             dma((14,)), dma((2 * slots,)), dma((14,)), dma((2 * slots,)),
             dma((4,)), dma((4,)), dma((6,)), dma((6,)),
@@ -606,9 +710,9 @@
             vmem_limit_bytes=58 * 2**20, collective_id=0, has_side_effects=True
         ),
     )(
-        resid, mixer_in, log_step, decay_real, frequency,
-        input_matrix.reshape(2, width, -1), output_matrix.reshape(2, channels, states),
-        skip_gain.reshape(1, -1), value_weight, gate_weight, norm_gain.reshape(1, -1), up_weight, down_weight,
+        resid, mixer_in, log_step.T, decay_real, frequency,
+        input_matrix.transpose(0, 1, 3, 2).reshape(2, channels, states), output_matrix.reshape(2, channels, states),
+        skip_gain.reshape(1, -1), norm_gain.reshape(1, -1), value_weight, gate_weight, up_weight, down_weight,
     )
 
 

time: 80.6 us -> 69 us (0.86); the launches traced: 79.4 us -> 68.9 us
  Pallas kernels: 73.9 us -> 67.2 us
  local copies, waits for them, and re-layouts: 5.46 us -> 1.62 us
    pallas_call x1, Pallas kernels: 73.9 us -> 67.2 us  [per_device(): pl.pallas_call(layer_kernel, out_shape=jax.ShapeDtypeStruct((tokens, chan...]
    unnamed x3 -> x1, local copies, waits for them, and re-layouts: 5.46 us -> 1.62 us
where the time goes in v3:
time: 69 us; the launch traced here: 68.9 us
  Pallas kernels  67.2 us (97%)
  local copies, waits for them, and re-layouts  1.62 us (2%)
    pallas_call x1, Pallas kernels, per_device(): pl.pallas_call(layer_kernel, out_shape=jax.ShapeDtypeStruct((tokens, chan...  67.2 us
    unnamed x1, local copies, waits for them, and re-layouts  1.62 us

profile of v3, /device:TPU:1, one launch (start us, length us, event | category | flops | bytes accessed | tf_op | source)
XLA Modules:
  0.0 68.9 jit_solution(17546295704845499072)
XLA Ops:
  0.0 67.2 %layer.1 = bf16[384,256]{1,0:T(8,128)(2,1)} custom-call(bf16[384,256]{1,0:T(8,128)(2,1)} %resid_hbm.1, bf16[384,256]{1,0:T(8,128)(2,1)} %u_hbm.1, f32[16,384]{1,0:T(8,128)} %bitcast.9, f32[16,64]{1,0:T(8,128)} %dr_hbm.1, f32[16,64]{1,0:T(8,128)} %fr_hbm.1, f32[2,256,64]{2,1,0:T(8,128)} %bitcast.7, f32[2,256,64]{2,1,0:T(8,128)} %bitcast.8, ...), custom_call_target="tpu_custom_call" | custom-call | tf_op jit(solution)/shard_map/layer/pallas_call | solution.py:681
  67.3 1.6 %copy.15 = bf16[384,256]{1,0:T(8,128)(2,1)} copy(bf16[384,256]{1,0:T(8,128)(2,1)} %layer.1) | data formatting | bytes 393216

commit v4 on v3

--- a/solution.py
+++ b/solution.py
@@ -216,84 +216,89 @@
 
 
 class Relay:
-    def __init__(self, buf, send_sem, recv_sem, y_first):
+    def __init__(self, buf, own, send_sem, recv_sem, y_first):
         here = lax.axis_index("sp")
         z, y = here // SIDE, lax.rem(here, SIDE)
         self.p, self.q = (y, z) if y_first else (z, y)
-        self.y_first = y_first
-        self.buf, self.send_sem, self.recv_sem = buf, send_sem, recv_sem
+        self.y_first, self.buf, self.own = y_first, buf, own
+        self.send_sem, self.recv_sem = send_sem, recv_sem
         self.rows = buf.shape[0] // (SIDE * SIDE)
-        self.started = []
+        self.sent = 0
 
     def index(self, dp, dq):
         p, q = around(self.p, dp), around(self.q, dq)
         return q * SIDE + p if self.y_first else p * SIDE + q
 
-    def copy(self, number, slot, half, target):
+    def group(self, dp, dq, half):
+        if dq == 0:
+            return 2 if dp == 2 else int((dp == -1) == (half == 1))
+        if dq == 2:
+            return 9
+        return 3 + dp % SIDE if (dq == -1) == (half == 0) else (7 if dq == -1 else 8)
+
+    def send(self, dp, dq, half, to_p, to_q, hbm=False):
         rows = self.rows // 2
+        slot = self.index(dp, dq)
         piece = self.buf.at[pl.ds(pl.multiple_of(slot * self.rows + half * rows, rows), rows), :]
+        seen = [(d + 1) % SIDE - 1 for d in (dp - to_p, dq - to_q)]
+        pltpu.make_async_remote_copy(
+            src_ref=self.own.at[half * rows : half * rows + rows, :] if hbm else piece,
+            dst_ref=piece,
+            send_sem=self.send_sem,
+            recv_sem=self.recv_sem.at[self.group(*seen, half)],
+            device_id={"sp": self.index(to_p, to_q), "tp": lax.axis_index("tp")},
+            device_id_type=AXES,
+        ).start()
+        self.sent += 1
+
+    def whole(self, count, group):
+        rows = self.buf.at[: count * self.rows // 2, :]
         return pltpu.make_async_remote_copy(
-            src_ref=piece,
-            dst_ref=piece,
-            send_sem=self.send_sem.at[number],
-            recv_sem=self.recv_sem.at[slot * 2 + half],
-            device_id={"sp": target, "tp": lax.axis_index("tp")},
+            src_ref=rows,
+            dst_ref=rows,
+            send_sem=self.send_sem,
+            recv_sem=self.recv_sem.at[group],
+            device_id={"sp": self.index(1, 0), "tp": lax.axis_index("tp")},
             device_id_type=AXES,
         )
 
-    def send(self, slot, half, dp, dq):
-        copy = self.copy(len(self.started), slot, half, self.index(dp, dq))
-        copy.start()
-        self.started.append(copy)
-
-    def arrived(self, dp, dq, half):
-        self.copy(0, self.index(dp, dq), half, self.index(1, 0)).wait_recv()
-
-    def start_p(self):
-        own = self.index(0, 0)
+    def arrived(self, group):
+        self.whole({7: 4, 8: 4, 9: 8}.get(group, 2), group).wait_recv()
+
+    def send_p(self):
         for k in range(2):
-            self.send(own, k, 1, 0)
-            self.send(own, 1 - k, -1, 0)
-
-    def send_q(self, slot, part=(0, 1)):
+            self.send(0, 0, k, 1, 0, True)
+            self.send(0, 0, 1 - k, -1, 0, True)
+
+    def send_q(self, dp, part=(0, 1), hbm=False):
         for k in part:
-            self.send(slot, k, 0, 1)
-            self.send(slot, 1 - k, 0, -1)
+            self.send(dp, 0, k, 0, 1, hbm)
+            self.send(dp, 0, 1 - k, 0, -1, hbm)
 
     def forward_p(self):
-        self.arrived(-1, 0, 0)
-        self.send(self.index(-1, 0), 0, 1, 0)
-        self.arrived(1, 0, 1)
-        self.send(self.index(1, 0), 1, -1, 0)
-
-    def serve_near(self):
-        self.arrived(-1, 0, 1)
-        self.send_q(self.index(-1, 0))
-        self.arrived(1, 0, 0)
-        self.send_q(self.index(1, 0))
-
-    def serve_far(self):
-        self.arrived(2, 0, 0)
-        self.arrived(2, 0, 1)
-        self.send_q(self.index(2, 0))
+        self.arrived(0)
+        self.send(-1, 0, 0, 1, 0)
+        self.send(1, 0, 1, -1, 0)
+
+    def near(self):
+        self.arrived(1)
+        self.send_q(-1)
+        self.send_q(1)
+
+    def far(self):
+        self.arrived(2)
+        self.send_q(2)
 
     def forward_q(self, dp):
-        self.arrived(dp, -1, 0)
-        self.send(self.index(dp, -1), 0, 0, 1)
-        self.arrived(dp, 1, 1)
-        self.send(self.index(dp, 1), 1, 0, -1)
+        self.arrived(3 + dp % SIDE)
+        self.send(dp, -1, 0, 0, 1)
+        self.send(dp, 1, 1, 0, -1)
 
     def finish(self, dq):
-        for dp in (0, -1, 1, 2):
-            if dq == 2:
-                self.arrived(dp, 2, 0)
-                self.arrived(dp, 2, 1)
-            elif dq:
-                self.arrived(dp, dq, 1 if dq == -1 else 0)
+        self.arrived({-1: 7, 1: 8, 2: 9}[dq])
 
     def drain(self):
-        for copy in self.started:
-            copy.wait_send()
+        self.whole(self.sent, 0).wait_send()
 
 
 class Gather:
@@ -301,64 +306,73 @@
         here = lax.axis_index("tp")
         self.x, self.core = here // 2, lax.rem(here, 2)
         self.buf, self.send_sem, self.recv_sem = buf, send_sem, recv_sem
-        self.started = []
+        self.sent = 0
 
     def slot(self, dx, other=False):
         core = 1 - self.core if other else self.core
         return around(self.x, dx) * 2 + core
 
-    def copy(self, number, slot, half, target):
+    def send(self, dx, half, to_x):
         rows = self.buf.shape[1] // 2
-        piece = self.buf.at[slot, half * rows : half * rows + rows, :]
-        return pltpu.make_async_remote_copy(
+        piece = self.buf.at[self.slot(dx), half * rows : half * rows + rows, :]
+        if to_x:
+            seen = (dx - to_x + 1) % SIDE - 1
+            group = 2 if seen == 2 else int((seen == -1) == (half == 1))
+            target = self.slot(to_x)
+        else:
+            group, target = 3 + dx % SIDE, self.slot(0, True)
+        pltpu.make_async_remote_copy(
             src_ref=piece,
             dst_ref=piece,
-            send_sem=self.send_sem.at[number],
-            recv_sem=self.recv_sem.at[slot * 2 + half],
+            send_sem=self.send_sem,
+            recv_sem=self.recv_sem.at[group],
             device_id={"sp": lax.axis_index("sp"), "tp": target},
             device_id_type=AXES,
+        ).start()
+        self.sent += 1
+
+    def whole(self, pieces, group):
+        rows = self.buf.at[pieces]
+        return pltpu.make_async_remote_copy(
+            src_ref=rows,
+            dst_ref=rows,
+            send_sem=self.send_sem,
+            recv_sem=self.recv_sem.at[group],
+            device_id={"sp": lax.axis_index("sp"), "tp": self.slot(1)},
+            device_id_type=AXES,
         )
 
-    def send(self, dx, half, target):
-        copy = self.copy(len(self.started), self.slot(dx), half, target)
-        copy.start()
-        self.started.append(copy)
-
-    def arrived(self, dx, half, other=False):
-        self.copy(0, self.slot(dx, other), half, self.slot(1)).wait_recv()
+    def arrived(self, group):
+        self.whole(0, group).wait_recv()
 
     def start(self):
         for k in range(2):
-            self.send(0, k, self.slot(1))
-            self.send(0, 1 - k, self.slot(-1))
+            self.send(0, k, 1)
+            self.send(0, 1 - k, -1)
         for k in range(2):
-            self.send(0, k, self.slot(0, True))
-
-    def serve_near(self):
-        self.arrived(-1, 0)
-        self.send(-1, 0, self.slot(1))
-        self.arrived(1, 1)
-        self.send(1, 1, self.slot(-1))
-        self.send(-1, 0, self.slot(0, True))
-        self.send(1, 1, self.slot(0, True))
-        self.arrived(-1, 1)
-        self.send(-1, 1, self.slot(0, True))
-        self.arrived(1, 0)
-        self.send(1, 0, self.slot(0, True))
-
-    def serve_far(self):
-        for k in range(2):
-            self.arrived(2, k)
-            self.send(2, k, self.slot(0, True))
+            self.send(0, k, 0)
+
+    def near(self):
+        self.arrived(0)
+        self.send(-1, 0, 1)
+        self.send(1, 1, -1)
+        self.send(-1, 0, 0)
+        self.send(1, 1, 0)
+        self.arrived(1)
+        self.send(-1, 1, 0)
+        self.send(1, 0, 0)
+
+    def far(self):
+        self.arrived(2)
+        self.send(2, 0, 0)
+        self.send(2, 1, 0)
 
     def finish(self):
-        for dx in (0, -1, 1, 2):
-            for k in range(2):
-                self.arrived(dx, k, True)
+        for dx in range(SIDE):
+            self.arrived(3 + dx)
 
     def drain(self):
-        for copy in self.started:
-            copy.wait_send()
+        self.whole(slice(0, self.sent // 2), 0).wait_send()
 
 
 class Phases:
@@ -380,18 +394,17 @@
     up_all, down_all, vg, dec_re, dec_im, feed_re, feed_im, step_wide, rows, ends, total, totals, carry,
     uperm, wout, states, mixed_all, upd_all, normed, glu, raised, hidden, stage_pair, from_pair, mine,
     stage_far, stage_right, stage_left, relay_left, relay_right, from_left, from_right,
-    local_sem, round_sem, up_send, up_recv, down_send, down_recv, tot_send, tot_recv,
-    mix_send, mix_recv, upd_send, upd_recv, pair_send, pair_recv, sum_send, sum_recv,
+    local_sem, round_sem, ring_send, ring_recv, tot_send, tot_recv, sum_send, sum_recv,
 ):
     phase = Phases()
     here, lane = lax.axis_index("sp"), lax.axis_index("tp")
     planes = SIDE * SIDE
     tokens, piece = resid_ref.shape
     half = tokens // 2
-    up = Relay(up_all, up_send, up_recv, True)
-    down = Relay(down_all, down_send, down_recv, False)
-    mix = Gather(mixed_all, mix_send, mix_recv)
-    upd = Gather(upd_all, upd_send, upd_recv)
+    up = Relay(up_all, up_ref, ring_send.at[0], ring_recv.at[0], True)
+    down = Relay(down_all, down_ref, ring_send.at[1], ring_recv.at[1], False)
+    mix = Gather(mixed_all, ring_send.at[2], ring_recv.at[2])
+    upd = Gather(upd_all, ring_send.at[3], ring_recv.at[3])
     right, left, partner = mix.slot(1), mix.slot(-1), mix.slot(0, True)
     near_planes = [up.index(*by) for by in ((1, 0), (-1, 0), (0, 1), (0, -1))]
 
@@ -412,16 +425,13 @@
     local = [pltpu.make_async_copy(src, dst, local_sem.at[k]) for k, (src, dst) in enumerate(moves)]
     for copy in local:
         copy.start()
-    local[0].wait()
-    local[1].wait()
     phase("barrier")
     pl.semaphore_wait(barrier, 7)
     phase("start_p")
-    own_up, own_down = up.index(0, 0), down.index(0, 0)
-    up.start_p()
-    down.start_p()
-    up.send_q(own_up, (0,))
-    down.send_q(own_down, (0,))
+    up.send_p()
+    down.send_p()
+    up.send_q(0, (0,), True)
+    down.send_q(0, (0,), True)
 
     def greet(number):
         for target in near_planes:
@@ -466,11 +476,13 @@
     up.forward_p()
     down.forward_p()
     phase("send_q")
-    up.send_q(own_up, (1,))
-    down.send_q(own_down, (1,))
+    local[0].wait()
+    local[1].wait()
+    up.send_q(0, (1,))
+    down.send_q(0, (1,))
     phase("serve_near")
-    up.serve_near()
-    down.serve_near()
+    up.near()
+    down.near()
 
     phase("fold")
 
@@ -493,14 +505,14 @@
     phase("mix_start")
     mix.start()
     phase("serve_far")
-    up.serve_far()
-    down.serve_far()
+    up.far()
+    down.far()
     up.forward_q(0)
     down.forward_q(0)
     phase("mix_near")
-    mix.serve_near()
+    mix.near()
     phase("mix_far")
-    mix.serve_far()
+    mix.far()
     phase("fq_minus")
     up.forward_q(-1)
     down.forward_q(-1)
@@ -527,12 +539,12 @@
     up.forward_q(1)
     down.forward_q(1)
     phase("upd_near")
-    upd.serve_near()
+    upd.near()
     phase("fq_far")
     up.forward_q(2)
     down.forward_q(2)
     phase("upd_far")
-    upd.serve_far()
+    upd.far()
     phase("upd_finish")
     upd.finish()
 
@@ -550,103 +562,89 @@
             upd_all[s].astype(f32) * inv_rms * gain_ref[:, at]
         ).astype(bf16)
 
-    width = hidden.shape[1]
     depth = normed.shape[2]
     for k, dq in enumerate((0, -1, 1, 2)):
-        phase(f"up_wait{k}")
-        up.finish(dq)
+        if k:
+            phase(f"up_wait{k}")
+            up.finish(dq)
         phase(f"up_mm{k}")
         group = around(up.q, dq)
-        deep = pl.ds(pl.multiple_of(group * depth, depth), depth)
-
-        def up_step(n, _):
-            at = pl.ds(pl.multiple_of(n * piece, piece), piece)
-            product = dot(normed[group], up_all[deep, at])
-            if k:
-                product = product + raised[:, at]
-            if k < 3:
-                raised[:, at] = product
-            else:
-                active = jnp.maximum(product, 0.0)
-                hidden[:, at] = (active * active).astype(bf16)
-            return 0
-
-        lax.fori_loop(0, width // piece, up_step, 0)
+        product = dot(normed[group], up_all[pl.ds(pl.multiple_of(group * depth, depth), depth), :])
+        if k == 0:
+            raised[...] = product
+        elif k < 3:
+            raised[...] += product
+        else:
+            active = jnp.maximum(raised[...] + product, 0.0)
+            hidden[...] = (active * active).astype(bf16)
     phase("down_finish")
-    for dq in (0, -1, 1, 2):
+    for dq in (-1, 1, 2):
         down.finish(dq)
 
-    def product(slot):
-        at = pl.ds(pl.multiple_of(slot * piece, piece), piece)
-        return dot_t(hidden[...], down_all[at, :])
-
-    def sum_copy(number, src, dst, target, send_sem, recv_sem):
+    def sum_copy(number, src, dst, target):
         return pltpu.make_async_remote_copy(
             src_ref=src,
             dst_ref=dst,
-            send_sem=send_sem.at[number],
-            recv_sem=recv_sem.at[number],
+            send_sem=sum_send.at[number],
+            recv_sem=sum_recv.at[number],
             device_id={"sp": here, "tp": target},
             device_id_type=AXES,
         )
 
     order = (2, 1, -1, 0)
-    pairs = [
-        sum_copy(k, stage_pair.at[k], from_pair.at[k], partner, pair_send, pair_recv) for k in range(len(order))
+    sums = [
+        sum_copy(0, stage_far.at[:half, :], relay_left, right),
+        sum_copy(1, stage_far.at[half:, :], relay_right, left),
+        sum_copy(2, stage_right.at[half:, :], from_left.at[half:, :], right),
+        sum_copy(3, stage_left.at[:half, :], from_right.at[:half, :], left),
+        sum_copy(4, stage_right.at[:half, :], from_left.at[:half, :], right),
+        sum_copy(5, stage_left.at[half:, :], from_right.at[half:, :], left),
     ]
-    sums = [
-        sum_copy(0, stage_far.at[:half, :], relay_left, right, sum_send, sum_recv),
-        sum_copy(1, stage_far.at[half:, :], relay_right, left, sum_send, sum_recv),
-        sum_copy(2, stage_right.at[half:, :], from_left.at[half:, :], right, sum_send, sum_recv),
-        sum_copy(3, stage_left.at[:half, :], from_right.at[:half, :], left, sum_send, sum_recv),
-        sum_copy(4, stage_right.at[:half, :], from_left.at[:half, :], right, sum_send, sum_recv),
-        sum_copy(5, stage_left.at[half:, :], from_right.at[half:, :], left, sum_send, sum_recv),
-    ]
-
-    def pair_step(k):
-        stage_pair[k] = product(mix.slot(order[k], True)).astype(bf16)
+    pairs = [sum_copy(6 + k, stage_pair.at[k], from_pair.at[k], partner) for k in range(len(order))]
+    own_cols = pl.ds(pl.multiple_of(mix.core * piece, piece), piece)
+    other_cols = pl.ds(pl.multiple_of((1 - mix.core) * piece, piece), piece)
+
+    def step(k):
+        at = pl.ds(pl.multiple_of(around(mix.x, order[k]) * 2 * piece, 2 * piece), 2 * piece)
+        mine[k] = dot_t(hidden[...], down_all[at, :])
+        stage_pair[k] = mine[k, :, other_cols].astype(bf16)
         pairs[k].start()
-
-    def own_step(k):
-        mine[k] = product(mix.slot(order[k]))
 
     def pair_sum(k):
         pairs[k].wait_recv()
-        return mine[k] + from_pair[k].astype(f32)
+        return mine[k, :, own_cols] + from_pair[k].astype(f32)
 
     phase("products")
-    pair_step(0)
-    own_step(0)
-    pair_step(1)
-    pair_step(2)
+    step(0)
+    step(1)
     phase("far")
     stage_far[...] = pair_sum(0).astype(bf16)
     sums[0].start()
     sums[1].start()
     phase("near")
-    own_step(1)
-    own_step(2)
-    mine[1] = pair_sum(1)
-    stage_right[half:, :] = mine[1, half:, :].astype(bf16)
+    step(2)
+    near = pair_sum(1)
+    stage_right[half:, :] = near[half:].astype(bf16)
     sums[2].start()
-    mine[2] = pair_sum(2)
-    stage_left[:half, :] = mine[2, :half, :].astype(bf16)
+    mine[1, :half, own_cols] = near[:half]
+    step(3)
+    near = pair_sum(2)
+    stage_left[:half, :] = near[:half].astype(bf16)
     sums[3].start()
-    pair_step(3)
-    own_step(3)
+    mine[2, half:, own_cols] = near[half:]
+    mine[3, :, own_cols] = pair_sum(3) + upd_all[lane].astype(f32)
     phase("relay")
     sums[0].wait_recv()
-    stage_right[:half, :] = (mine[1, :half, :] + relay_left[...].astype(f32)).astype(bf16)
+    stage_right[:half, :] = (mine[1, :half, own_cols] + relay_left[...].astype(f32)).astype(bf16)
     sums[4].start()
     sums[1].wait_recv()
-    stage_left[half:, :] = (mine[2, half:, :] + relay_right[...].astype(f32)).astype(bf16)
+    stage_left[half:, :] = (mine[2, half:, own_cols] + relay_right[...].astype(f32)).astype(bf16)
     sums[5].start()
-    mine[3] = pair_sum(3) + upd_all[lane].astype(f32)
     phase("sum_wait")
     for k in range(2, 6):
         sums[k].wait_recv()
     phase("result")
-    result = mine[3] + (from_left[...].astype(f32) + from_right[...].astype(f32))
+    result = mine[3, :, own_cols] + (from_left[...].astype(f32) + from_right[...].astype(f32))
     out_ref[...] = result.astype(bf16)
 
     phase("drain")
@@ -698,12 +696,10 @@
             pltpu.VMEM((SIDE, tokens, features // SIDE), bf16), pltpu.VMEM((tokens, 2 * channels), f32),
             pltpu.VMEM((tokens, hidden), f32), pltpu.VMEM((tokens, hidden), bf16),
             pltpu.VMEM((4, tokens, channels), bf16), pltpu.VMEM((4, tokens, channels), bf16),
-            pltpu.VMEM((4, tokens, channels), f32),
+            pltpu.VMEM((4, tokens, 2 * channels), f32),
             block, block, block, halves, halves, block, block,
-            dma((13,)), pltpu.SemaphoreType.REGULAR((3,)), dma((30,)), dma((2 * planes,)), dma((30,)), dma((2 * planes,)),
-            dma((planes,)), dma((planes,)),
-            dma((14,)), dma((2 * slots,)), dma((14,)), dma((2 * slots,)),
-            dma((4,)), dma((4,)), dma((6,)), dma((6,)),
+            dma((13,)), pltpu.SemaphoreType.REGULAR((3,)), dma((4,)), dma((4, 10)),
+            dma((planes,)), dma((planes,)), dma((10,)), dma((10,)),
         ],
         name="layer",
         compiler_params=pltpu.CompilerParams(

time: 69 us -> 68.3 us (0.990)
  no operation moved by 1% of the time
where the time goes in v4:
time: 68.3 us; the launch traced here: 68.2 us
  Pallas kernels  66.6 us (98%)
  local copies, waits for them, and re-layouts  1.62 us (2%)
    pallas_call x1, Pallas kernels, per_device(): pl.pallas_call(layer_kernel, out_shape=jax.ShapeDtypeStruct((tokens, chan...  66.6 us
    unnamed x1, local copies, waits for them, and re-layouts  1.62 us

profile of v4, /device:TPU:1, one launch (start us, length us, event | category | flops | bytes accessed | tf_op | source)
XLA Modules:
  0.0 68.2 jit_solution(7529612892699171738)
XLA Ops:
  0.0 66.6 %layer.1 = bf16[384,256]{1,0:T(8,128)(2,1)} custom-call(bf16[384,256]{1,0:T(8,128)(2,1)} %resid_hbm.1, bf16[384,256]{1,0:T(8,128)(2,1)} %u_hbm.1, f32[16,384]{1,0:T(8,128)} %bitcast.9, f32[16,64]{1,0:T(8,128)} %dr_hbm.1, f32[16,64]{1,0:T(8,128)} %fr_hbm.1, f32[2,256,64]{2,1,0:T(8,128)} %bitcast.7, f32[2,256,64]{2,1,0:T(8,128)} %bitcast.8, ...), custom_call_target="tpu_custom_call" | custom-call | tf_op jit(solution)/shard_map/layer/pallas_call | solution.py:679
  66.6 1.6 %copy.15 = bf16[384,256]{1,0:T(8,128)(2,1)} copy(bf16[384,256]{1,0:T(8,128)(2,1)} %layer.1) | data formatting | bytes 393216

commit v5 on v4

--- a/solution.py
+++ b/solution.py
@@ -216,37 +216,37 @@
 
 
 class Relay:
-    def __init__(self, buf, own, send_sem, recv_sem, y_first):
+    def __init__(self, buf, first, rows, send_sem, recv_sem, own=None):
         here = lax.axis_index("sp")
-        z, y = here // SIDE, lax.rem(here, SIDE)
-        self.p, self.q = (y, z) if y_first else (z, y)
-        self.y_first, self.buf, self.own = y_first, buf, own
+        self.zy = here // SIDE, lax.rem(here, SIDE)
+        self.buf, self.first, self.rows, self.own = buf, first, rows, own
+        self.shard = buf.shape[0] // (SIDE * SIDE)
         self.send_sem, self.recv_sem = send_sem, recv_sem
-        self.rows = buf.shape[0] // (SIDE * SIDE)
         self.sent = 0
 
-    def index(self, dp, dq):
-        p, q = around(self.p, dp), around(self.q, dq)
-        return q * SIDE + p if self.y_first else p * SIDE + q
+    def index(self, side, dp, dq):
+        dz, dy = (dq, dp) if side == 0 else (dp, dq)
+        return around(self.zy[0], dz) * SIDE + around(self.zy[1], dy)
 
     def group(self, dp, dq, half):
         if dq == 0:
             return 2 if dp == 2 else int((dp == -1) == (half == 1))
-        if dq == 2:
-            return 9
-        return 3 + dp % SIDE if (dq == -1) == (half == 0) else (7 if dq == -1 else 8)
-
-    def send(self, dp, dq, half, to_p, to_q, hbm=False):
-        rows = self.rows // 2
-        slot = self.index(dp, dq)
-        piece = self.buf.at[pl.ds(pl.multiple_of(slot * self.rows + half * rows, rows), rows), :]
+        return 3 + dp % SIDE if dq != 2 and (dq == -1) == (half == 0) else 7
+
+    def send(self, side, dp, dq, half, to_p, to_q):
+        width = self.buf.shape[1] // 2
+        cols = slice(half * width, half * width + width)
+        row = pl.multiple_of(self.index(side, dp, dq) * self.shard + side * self.rows, self.rows)
+        piece = self.buf.at[pl.ds(row, self.rows), cols]
+        own = self.own is not None and dp == 0 and dq == 0
+        first = self.first + side * self.rows
         seen = [(d + 1) % SIDE - 1 for d in (dp - to_p, dq - to_q)]
         pltpu.make_async_remote_copy(
-            src_ref=self.own.at[half * rows : half * rows + rows, :] if hbm else piece,
+            src_ref=self.own.at[first : first + self.rows, cols] if own else piece,
             dst_ref=piece,
             send_sem=self.send_sem,
             recv_sem=self.recv_sem.at[self.group(*seen, half)],
-            device_id={"sp": self.index(to_p, to_q), "tp": lax.axis_index("tp")},
+            device_id={"sp": self.index(side, to_p, to_q), "tp": lax.axis_index("tp")},
             device_id_type=AXES,
         ).start()
         self.sent += 1
@@ -258,27 +258,30 @@
             dst_ref=rows,
             send_sem=self.send_sem,
             recv_sem=self.recv_sem.at[group],
-            device_id={"sp": self.index(1, 0), "tp": lax.axis_index("tp")},
+            device_id={"sp": self.index(0, 1, 0), "tp": lax.axis_index("tp")},
             device_id_type=AXES,
         )
 
     def arrived(self, group):
-        self.whole({7: 4, 8: 4, 9: 8}.get(group, 2), group).wait_recv()
+        self.whole(32 if group == 7 else 4, group).wait_recv()
 
     def send_p(self):
         for k in range(2):
-            self.send(0, 0, k, 1, 0, True)
-            self.send(0, 0, 1 - k, -1, 0, True)
-
-    def send_q(self, dp, part=(0, 1), hbm=False):
-        for k in part:
-            self.send(dp, 0, k, 0, 1, hbm)
-            self.send(dp, 0, 1 - k, 0, -1, hbm)
+            for side in range(2):
+                self.send(side, 0, 0, k, 1, 0)
+                self.send(side, 0, 0, 1 - k, -1, 0)
+
+    def send_q(self, dp):
+        for k in range(2):
+            for side in range(2):
+                self.send(side, dp, 0, k, 0, 1)
+                self.send(side, dp, 0, 1 - k, 0, -1)
 
     def forward_p(self):
         self.arrived(0)
-        self.send(-1, 0, 0, 1, 0)
-        self.send(1, 0, 1, -1, 0)
+        for side in range(2):
+            self.send(side, -1, 0, 0, 1, 0)
+            self.send(side, 1, 0, 1, -1, 0)
 
     def near(self):
         self.arrived(1)
@@ -291,11 +294,12 @@
 
     def forward_q(self, dp):
         self.arrived(3 + dp % SIDE)
-        self.send(dp, -1, 0, 0, 1)
-        self.send(dp, 1, 1, 0, -1)
-
-    def finish(self, dq):
-        self.arrived({-1: 7, 1: 8, 2: 9}[dq])
+        for side in range(2):
+            self.send(side, dp, -1, 0, 0, 1)
+            self.send(side, dp, 1, 1, 0, -1)
+
+    def finish(self):
+        self.arrived(7)
 
     def drain(self):
         self.whole(self.sent, 0).wait_send()
@@ -308,42 +312,43 @@
         self.buf, self.send_sem, self.recv_sem = buf, send_sem, recv_sem
         self.sent = 0
 
-    def slot(self, dx, other=False):
-        core = 1 - self.core if other else self.core
-        return around(self.x, dx) * 2 + core
+    def device(self, dx, other=False):
+        return around(self.x, dx) * 2 + (1 - self.core if other else self.core)
+
+    def cols(self, core):
+        width = self.buf.shape[2] // 2
+        return pl.ds(pl.multiple_of(core * width, width), width)
 
     def send(self, dx, half, to_x):
         rows = self.buf.shape[1] // 2
-        piece = self.buf.at[self.slot(dx), half * rows : half * rows + rows, :]
+        piece = self.buf.at[around(self.x, dx), half * rows : half * rows + rows, self.cols(self.core)]
         if to_x:
             seen = (dx - to_x + 1) % SIDE - 1
             group = 2 if seen == 2 else int((seen == -1) == (half == 1))
-            target = self.slot(to_x)
         else:
-            group, target = 3 + dx % SIDE, self.slot(0, True)
+            group = 3 + dx % SIDE
         pltpu.make_async_remote_copy(
             src_ref=piece,
             dst_ref=piece,
             send_sem=self.send_sem,
             recv_sem=self.recv_sem.at[group],
-            device_id={"sp": lax.axis_index("sp"), "tp": target},
+            device_id={"sp": lax.axis_index("sp"), "tp": self.device(to_x, not to_x)},
             device_id_type=AXES,
         ).start()
         self.sent += 1
 
-    def whole(self, pieces, group):
-        rows = self.buf.at[pieces]
+    def whole(self, rows, group):
         return pltpu.make_async_remote_copy(
             src_ref=rows,
             dst_ref=rows,
             send_sem=self.send_sem,
             recv_sem=self.recv_sem.at[group],
-            device_id={"sp": lax.axis_index("sp"), "tp": self.slot(1)},
+            device_id={"sp": lax.axis_index("sp"), "tp": self.device(1)},
             device_id_type=AXES,
         )
 
     def arrived(self, group):
-        self.whole(0, group).wait_recv()
+        self.whole(self.buf.at[0, :, : self.buf.shape[2] // 2], group).wait_recv()
 
     def start(self):
         for k in range(2):
@@ -367,12 +372,11 @@
         self.send(2, 0, 0)
         self.send(2, 1, 0)
 
-    def finish(self):
-        for dx in range(SIDE):
-            self.arrived(3 + dx)
+    def across(self, dx):
+        self.arrived(3 + dx % SIDE)
 
     def drain(self):
-        self.whole(slice(0, self.sent // 2), 0).wait_send()
+        self.whole(self.buf.at[:, : self.buf.shape[1] * self.sent // 16, :], 0).wait_send()
 
 
 class Phases:
@@ -391,22 +395,25 @@
     resid_hbm, u_hbm, ls_hbm, dr_hbm, fr_hbm, bm_hbm, cm_hbm, skip_hbm, gain_hbm, vw_ref, gw_ref, up_ref, down_ref,
     out_ref,
     resid_ref, u_ref, ls_ref, dr_ref, fr_ref, bm_ref, cm_ref, skip_ref, gain_ref,
-    up_all, down_all, vg, dec_re, dec_im, feed_re, feed_im, step_wide, rows, ends, total, totals, carry,
-    uperm, wout, states, mixed_all, upd_all, normed, glu, raised, hidden, stage_pair, from_pair, mine,
-    stage_far, stage_right, stage_left, relay_left, relay_right, from_left, from_right,
-    local_sem, round_sem, ring_send, ring_recv, tot_send, tot_recv, sum_send, sum_recv,
+    up_all, down_first, down_last, vg, dec_re, dec_im, feed_re, feed_im, step_wide, rows, ends, total, totals, carry,
+    uperm, wout, states, mixed_all, upd_all, glu, raised, squares, hidden,
+    products, stage_far, relay_in, stage_near, from_near, kept, stage_own, from_own, own_part,
+    local_sem, round_sem, ring_send, ring_recv, tot_send, tot_recv, cross_send, cross_recv, sum_send, sum_recv,
 ):
     phase = Phases()
     here, lane = lax.axis_index("sp"), lax.axis_index("tp")
     planes = SIDE * SIDE
     tokens, piece = resid_ref.shape
     half = tokens // 2
-    up = Relay(up_all, up_ref, ring_send.at[0], ring_recv.at[0], True)
-    down = Relay(down_all, down_ref, ring_send.at[1], ring_recv.at[1], False)
-    mix = Gather(mixed_all, ring_send.at[2], ring_recv.at[2])
-    upd = Gather(upd_all, ring_send.at[3], ring_recv.at[3])
-    right, left, partner = mix.slot(1), mix.slot(-1), mix.slot(0, True)
-    near_planes = [up.index(*by) for by in ((1, 0), (-1, 0), (0, 1), (0, -1))]
+    shard = up_ref.shape[0]
+    mix = Gather(mixed_all, ring_send.at[3], ring_recv.at[3])
+    upd = Gather(upd_all, ring_send.at[4], ring_recv.at[4])
+    right, left, partner = mix.device(1), mix.device(-1), mix.device(0, True)
+
+    up = Relay(up_all, 0, shard // 2, ring_send.at[0], ring_recv.at[0], up_ref)
+    first = Relay(down_first, 0, shard // 8, ring_send.at[1], ring_recv.at[1])
+    last = Relay(down_last, 0, shard // 8, ring_send.at[2], ring_recv.at[2])
+    near_planes = [up.index(0, *by) for by in ((1, 0), (-1, 0), (0, 1), (0, -1))]
 
     phase("signal")
     barrier = pltpu.get_barrier_semaphore()
@@ -415,10 +422,33 @@
     for target in (right, left, partner):
         pl.semaphore_signal(barrier, inc=1, device_id={"sp": here, "tp": target}, device_id_type=AXES)
 
-    own_rows = pl.ds(pl.multiple_of(here * up.rows, up.rows), up.rows)
+    own_up = pl.ds(pl.multiple_of(here * shard, shard), shard)
+    slim, width = shard // 4, up_ref.shape[1]
+    own_down = pl.ds(pl.multiple_of(here * slim, slim), slim)
+    own_units = pl.ds(pl.multiple_of(mix.core * width, width), width)
+
+    def down_rows(core, k):
+        return down_ref.at[pl.ds(pl.multiple_of(core * 2 * slim + k * slim, slim), slim), :]
+
+    def cross_copy(number, src, dst):
+        return pltpu.make_async_remote_copy(
+            src_ref=src,
+            dst_ref=dst,
+            send_sem=cross_send.at[number],
+            recv_sem=cross_recv.at[number],
+            device_id={"sp": here, "tp": partner},
+            device_id_type=AXES,
+        )
+
+    crossing = [
+        cross_copy(k, down_rows(1 - mix.core, k), buf.at[own_down, own_units])
+        for k, buf in enumerate((down_first, down_last))
+    ]
     moves = (
-        (up_ref, up_all.at[own_rows, :]), (down_ref, down_all.at[own_rows, :]),
         (u_hbm, u_ref), (dr_hbm, dr_ref), (fr_hbm, fr_ref), (ls_hbm, ls_ref), (bm_hbm, bm_ref), (cm_hbm, cm_ref),
+        (up_ref, up_all.at[own_up, :]),
+        (down_rows(mix.core, 0), down_first.at[own_down, own_units]),
+        (down_rows(mix.core, 1), down_last.at[own_down, own_units]),
         (skip_hbm, skip_ref), (vw_ref, vg.at[:, :piece]), (gw_ref, vg.at[:, piece:]),
         (resid_hbm, resid_ref), (gain_hbm, gain_ref),
     )
@@ -429,9 +459,9 @@
     pl.semaphore_wait(barrier, 7)
     phase("start_p")
     up.send_p()
-    down.send_p()
-    up.send_q(0, (0,), True)
-    down.send_q(0, (0,), True)
+    up.send_q(0)
+    for copy in crossing:
+        copy.start()
 
     def greet(number):
         for target in near_planes:
@@ -440,7 +470,7 @@
             )
 
     greet(0)
-    for copy in local[2:8]:
+    for copy in local[:6]:
         copy.wait()
     phase("prepare")
     prepare(u_ref, ls_ref, dr_ref, fr_ref, bm_ref, cm_ref, uperm, step_wide, feed_re, feed_im, rows, wout)
@@ -472,17 +502,10 @@
         def _():
             total_copy(by, here, lax.rem(here + by, planes)).start()
 
-    phase("forward_p")
+    phase("serve1")
     up.forward_p()
-    down.forward_p()
-    phase("send_q")
-    local[0].wait()
-    local[1].wait()
-    up.send_q(0, (1,))
-    down.send_q(0, (1,))
-    phase("serve_near")
     up.near()
-    down.near()
+    up.forward_q(0)
 
     phase("fold")
 
@@ -497,155 +520,256 @@
     h_re, h_im = lax.fori_loop(0, here, fold, (zero, zero))
     carry[0:8, :] = h_re
     carry[8:16, :] = h_im
+    phase("serve2")
+    up.far()
+    for copy in local[6:9]:
+        copy.wait()
+    for copy in crossing:
+        copy.wait_recv()
+    first.send_p()
     phase("second_pass")
     second_pass(dec_re, dec_im, feed_re, feed_im, ends, carry, states)
-    local[8].wait()
+    local[9].wait()
     phase("read_out")
-    mixed_all[lane] = read_out(states, wout, uperm, skip_ref)
+    own_cols = mix.cols(mix.core)
+    mixed_all[mix.x, :, own_cols] = read_out(states, wout, uperm, skip_ref)
     phase("mix_start")
     mix.start()
-    phase("serve_far")
-    up.far()
-    down.far()
-    up.forward_q(0)
-    down.forward_q(0)
+
+    depth = 2 * piece
+
+    def glu_part(chip, core=None):
+        if core is None:
+            lhs, at = mixed_all[chip], pl.ds(pl.multiple_of(chip * depth, depth), depth)
+        else:
+            lhs, at = mixed_all[chip, :, mix.cols(core)], pl.ds(pl.multiple_of((chip * 2 + core) * piece, piece), piece)
+        return dot(lhs, vg[at, :])
+
+    phase("mix_own")
+    for copy in local[10:]:
+        copy.wait()
+    mix.across(0)
+    glu[...] = glu_part(mix.x)
+    phase("serve3")
+    up.forward_q(-1)
+    up.forward_q(1)
+    first.send_q(0)
     phase("mix_near")
     mix.near()
+    phase("serve4")
+    up.forward_q(2)
+    phase("mix_left")
+    mix.across(-1)
+    glu[...] += glu_part(around(mix.x, -1))
+    phase("mix_right")
+    mix.across(1)
+    glu[...] += glu_part(around(mix.x, 1))
     phase("mix_far")
     mix.far()
-    phase("fq_minus")
-    up.forward_q(-1)
-    down.forward_q(-1)
-    phase("mix_finish")
-    mix.finish()
-
-    phase("glu")
-    for copy in local[9:]:
-        copy.wait()
-    glu[...] = jnp.zeros_like(glu)
-
-    def glu_step(s, _):
-        at = pl.ds(pl.multiple_of(s * piece, piece), piece)
-        glu[...] += dot(mixed_all[s], vg[at, :])
-        return 0
-
-    slots = mixed_all.shape[0]
-    lax.fori_loop(0, slots, glu_step, 0)
+    phase("mix_last")
+    far_chip = around(mix.x, 2)
+    glu[...] += glu_part(far_chip, mix.core)
+    mix.across(2)
+    glu[...] += glu_part(far_chip, 1 - mix.core)
+    phase("updated")
     updated = (resid_ref[...].astype(f32) + glu[:, :piece] * jax.nn.sigmoid(glu[:, piece:])).astype(bf16)
-    upd_all[lane] = updated
+    upd_all[upd.x, :, own_cols] = updated
     phase("upd_start")
     upd.start()
-    phase("fq_plus")
-    up.forward_q(1)
-    down.forward_q(1)
+    phase("serve5")
+    first.forward_p()
+    first.near()
+    last.send_p()
+
+    def up_part(chip, start, core=None):
+        if core is None:
+            wide, at = upd_all[chip], pl.ds(pl.multiple_of(chip * depth, depth), depth)
+        else:
+            wide, at = upd_all[chip, :, upd.cols(core)], pl.ds(pl.multiple_of((chip * 2 + core) * piece, piece), piece)
+        wide = wide.astype(f32)
+        square = wide * wide
+        square = sum(square[:, 128 * k : 128 * k + 128] for k in range(square.shape[1] // 128))
+        product = dot((wide * gain_ref[:, at]).astype(bf16), up_all[at, :])
+        if start:
+            squares[...] = square
+            raised[...] = product
+        else:
+            squares[...] += square
+            raised[...] += product
+
+    phase("up_wait")
+    up.finish()
+    phase("upd_own")
+    upd.across(0)
+    up_part(upd.x, True)
+    phase("serve6")
+    first.forward_q(0)
+    first.far()
+    last.send_q(0)
     phase("upd_near")
     upd.near()
-    phase("fq_far")
-    up.forward_q(2)
-    down.forward_q(2)
+    phase("upd_left")
+    upd.across(-1)
+    last.forward_p()
+    up_part(around(upd.x, -1), False)
+    phase("serve7")
+    first.forward_q(-1)
+    first.forward_q(1)
+    phase("upd_right")
+    upd.across(1)
+    up_part(around(upd.x, 1), False)
+    phase("serve8")
+    first.forward_q(2)
+    last.near()
     phase("upd_far")
     upd.far()
-    phase("upd_finish")
-    upd.finish()
-
-    phase("norm")
-
-    def square_step(s, total):
-        wide = upd_all[s].astype(f32)
-        return total + jnp.sum(wide * wide, axis=1, keepdims=True)
-
-    squares = lax.fori_loop(0, slots, square_step, jnp.zeros((tokens, 1), f32))
-    inv_rms = lax.rsqrt(squares / (slots * piece) + rms_eps)
-    for s in range(slots):
-        at = slice(s * piece, s * piece + piece)
-        normed[s // 2, :, s % 2 * piece : s % 2 * piece + piece] = (
-            upd_all[s].astype(f32) * inv_rms * gain_ref[:, at]
-        ).astype(bf16)
-
-    depth = normed.shape[2]
-    for k, dq in enumerate((0, -1, 1, 2)):
-        if k:
-            phase(f"up_wait{k}")
-            up.finish(dq)
-        phase(f"up_mm{k}")
-        group = around(up.q, dq)
-        product = dot(normed[group], up_all[pl.ds(pl.multiple_of(group * depth, depth), depth), :])
-        if k == 0:
-            raised[...] = product
-        elif k < 3:
-            raised[...] += product
-        else:
-            active = jnp.maximum(raised[...] + product, 0.0)
-            hidden[...] = (active * active).astype(bf16)
-    phase("down_finish")
-    for dq in (-1, 1, 2):
-        down.finish(dq)
-
-    def sum_copy(number, src, dst, target):
-        return pltpu.make_async_remote_copy(
-            src_ref=src,
-            dst_ref=dst,
-            send_sem=sum_send.at[number],
-            recv_sem=sum_recv.at[number],
-            device_id={"sp": here, "tp": target},
-            device_id_type=AXES,
-        )
-
-    order = (2, 1, -1, 0)
-    sums = [
-        sum_copy(0, stage_far.at[:half, :], relay_left, right),
-        sum_copy(1, stage_far.at[half:, :], relay_right, left),
-        sum_copy(2, stage_right.at[half:, :], from_left.at[half:, :], right),
-        sum_copy(3, stage_left.at[:half, :], from_right.at[:half, :], left),
-        sum_copy(4, stage_right.at[:half, :], from_left.at[:half, :], right),
-        sum_copy(5, stage_left.at[half:, :], from_right.at[half:, :], left),
-    ]
-    pairs = [sum_copy(6 + k, stage_pair.at[k], from_pair.at[k], partner) for k in range(len(order))]
-    own_cols = pl.ds(pl.multiple_of(mix.core * piece, piece), piece)
-    other_cols = pl.ds(pl.multiple_of((1 - mix.core) * piece, piece), piece)
-
-    def step(k):
-        at = pl.ds(pl.multiple_of(around(mix.x, order[k]) * 2 * piece, 2 * piece), 2 * piece)
-        mine[k] = dot_t(hidden[...], down_all[at, :])
-        stage_pair[k] = mine[k, :, other_cols].astype(bf16)
-        pairs[k].start()
-
-    def pair_sum(k):
-        pairs[k].wait_recv()
-        return mine[k, :, own_cols] + from_pair[k].astype(f32)
-
-    phase("products")
-    step(0)
-    step(1)
-    phase("far")
-    stage_far[...] = pair_sum(0).astype(bf16)
-    sums[0].start()
-    sums[1].start()
-    phase("near")
-    step(2)
-    near = pair_sum(1)
-    stage_right[half:, :] = near[half:].astype(bf16)
-    sums[2].start()
-    mine[1, :half, own_cols] = near[:half]
-    step(3)
-    near = pair_sum(2)
-    stage_left[:half, :] = near[:half].astype(bf16)
-    sums[3].start()
-    mine[2, half:, own_cols] = near[half:]
-    mine[3, :, own_cols] = pair_sum(3) + upd_all[lane].astype(f32)
-    phase("relay")
-    sums[0].wait_recv()
-    stage_right[:half, :] = (mine[1, :half, own_cols] + relay_left[...].astype(f32)).astype(bf16)
-    sums[4].start()
-    sums[1].wait_recv()
-    stage_left[half:, :] = (mine[2, half:, own_cols] + relay_right[...].astype(f32)).astype(bf16)
-    sums[5].start()
-    phase("sum_wait")
-    for k in range(2, 6):
-        sums[k].wait_recv()
+    up_part(far_chip, False, upd.core)
+    phase("upd_last")
+    upd.across(2)
+    up_part(far_chip, False, 1 - upd.core)
+    phase("hidden")
+    inv_rms = lax.rsqrt(jnp.sum(squares[...], axis=1, keepdims=True) / (SIDE * depth) + rms_eps)
+    active = jnp.maximum(raised[...] * inv_rms, 0.0)
+    hidden[:, own_units] = (active * active).astype(bf16)
+    crossing.append(cross_copy(2, hidden.at[:, own_units], hidden.at[:, own_units]))
+    crossing[2].start()
+    phase("serve9")
+    last.far()
+    last.forward_q(0)
+
+    span = piece // 2
+    quarter = half // 2
+
+    def low_lanes(rows):
+        return lax.broadcasted_iota(jnp.int32, (rows, span), 1) < span // 2
+
+    def turned(value, by=None):
+        return pltpu.roll(value, span // 2 if by is None else by, 1)
+
+    def packed(value, core):
+        top, low = value[:quarter], value[quarter:]
+        if core == 0:
+            return jnp.where(low_lanes(quarter), top, turned(low))
+        return jnp.where(low_lanes(quarter), turned(top), low)
+
+    class Sum:
+        def __init__(self, k, buf):
+            self.k, self.buf = k, buf
+            self.relays = [
+                self.copy(0, j, stage_far.at[k, j], relay_in.at[k, j], target) for j, target in enumerate((right, left))
+            ]
+            self.own = self.copy(1, 2, stage_own.at[k], from_own.at[k], partner)
+            self.near = self.copy(2, 3, stage_near.at[k], from_near.at[k], right)
+
+        def copy(self, send, recv, src, dst, target):
+            return pltpu.make_async_remote_copy(
+                src_ref=src,
+                dst_ref=dst,
+                send_sem=sum_send.at[self.k, send],
+                recv_sem=sum_recv.at[self.k, recv],
+                device_id={"sp": here, "tp": target},
+                device_id_type=AXES,
+            )
+
+        def product(self, dx):
+            return products[:, pl.ds(pl.multiple_of(around(mix.x, dx) * span, span), span)]
+
+        def send_near(self, side, part, value):
+            chip = around(mix.x, 1 - 2 * side)
+            for core in range(2):
+                stage_near[self.k, side, core, part] = packed(value, core).astype(bf16)
+                self.copy(
+                    2, 3, stage_near.at[self.k, side, core, part], from_near.at[self.k, mix.core, side, part],
+                    chip * 2 + core,
+                ).start()
+
+        def start(self, *serve):
+            k = self.k
+            products[...] = dot_t(hidden[...], self.buf[...])
+            far = self.product(2).astype(bf16)
+            for j in range(2):
+                stage_far[k, j] = far[j * half : j * half + half]
+                self.relays[j].start()
+            near = self.product(1)
+            self.send_near(0, 1, near[half:])
+            kept[k, 0] = near[:half]
+            near = self.product(-1)
+            self.send_near(1, 0, near[:half])
+            kept[k, 1] = near[half:]
+            if serve:
+                serve[0]()
+            own = self.product(0)
+            for j in range(2):
+                both = [packed(own[j * half : j * half + half], core) for core in range(2)]
+                own_part[k, j] = jnp.where(mix.core == 0, both[0], both[1])
+                stage_own[k, j] = jnp.where(mix.core == 0, both[1], both[0]).astype(bf16)
+            self.own.start()
+            if serve:
+                serve[1]()
+
+        def relay(self):
+            for j in range(2):
+                self.relays[j].wait_recv()
+                self.send_near(j, j, kept[self.k, j] + relay_in[self.k, j].astype(f32))
+
+        def result(self):
+            k = self.k
+            self.own.wait_recv()
+            self.near.wait_recv()
+            found = []
+            for core in range(2):
+                rows = []
+                for j in range(2):
+                    here_part = jnp.where(mix.core == core, own_part[k, j], from_own[k, j].astype(f32))
+                    total = here_part + (from_near[k, core, 0, j].astype(f32) + from_near[k, core, 1, j].astype(f32))
+                    rows += [total, turned(total)]
+                found.append(jnp.concatenate(rows, axis=0))
+            return found
+
+        def drain(self):
+            self.own.wait_send()
+            self.near.wait_send()
+            self.copy(0, 0, stage_far.at[self.k], stage_far.at[self.k], right).wait_send()
+
+    phase("first_wait")
+    first.finish()
+    crossing[2].wait_recv()
+    phase("first_sum")
+    early, late = Sum(0, down_first), Sum(1, down_last)
+
+    def serve_near():
+        last.forward_q(-1)
+        last.forward_q(1)
+
+    def serve_far():
+        last.forward_q(2)
+
+    early.start(serve_near, serve_far)
+    phase("first_relay")
+    early.relay()
+    phase("last_wait")
+    last.finish()
+    phase("last_sum")
+    late.start()
+    phase("last_relay")
+    late.relay()
+    phase("first_result")
+    one = early.result()
+    phase("last_result")
+    two = late.result()
     phase("result")
-    result = mine[3, :, own_cols] + (from_left[...].astype(f32) + from_right[...].astype(f32))
-    out_ref[...] = result.astype(bf16)
+    lane_group = lax.broadcasted_iota(jnp.int32, (tokens, span), 1) // slim
+    blocks = []
+    for b in range(2):
+        block = None
+        for core in range(2):
+            for k, part in enumerate((one[core], two[core])):
+                place = core * 2 + k
+                moved = turned(part, (place - b) % 4 * slim) if place != b else part
+                block = moved if block is None else jnp.where(lane_group == place, moved, block)
+        blocks.append(block)
+    down_sum = jnp.concatenate(blocks, axis=1)
+    out_ref[...] = (upd_all[upd.x, :, own_cols].astype(f32) + down_sum).astype(bf16)
 
     phase("drain")
     for by in range(1, planes):
@@ -653,9 +777,9 @@
         def _():
             total_copy(by, here, lax.rem(here + by, planes)).wait_send()
 
-    for ring in (up, down, mix, upd):
-        ring.drain()
-    for copy in pairs + sums:
+    for part in (up, first, last, mix, upd, early, late):
+        part.drain()
+    for copy in crossing:
         copy.wait_send()
     phase(None)
 
@@ -670,11 +794,17 @@
     planes, slots = lax.axis_size("sp"), lax.axis_size("tp")
     features = slots * channels
     hidden = up_weight.shape[1]
+    span = channels // 2
     vmem = pl.BlockSpec(memory_space=pltpu.VMEM)
     hbm = pl.BlockSpec(memory_space=pl.ANY)
     wide = pltpu.VMEM((tokens, width), f32)
     block = pltpu.VMEM((tokens, channels), bf16)
-    halves = pltpu.VMEM((tokens // 2, channels), bf16)
+    halves = pltpu.VMEM((2, 2, tokens // 2, span), bf16)
+    packs = pltpu.VMEM((2, 2, tokens // 4, span), bf16)
+    near = pltpu.VMEM((2, 2, 2, 2, tokens // 4, span), bf16)
+    pieces = pltpu.VMEM((SIDE, tokens, 2 * channels), bf16)
+    matrix = pltpu.VMEM((2, channels, states), f32)
+    down = pltpu.VMEM((features // 4, 2 * hidden), bf16)
     dma = pltpu.SemaphoreType.DMA
     return pl.pallas_call(
         layer_kernel,
@@ -683,23 +813,19 @@
         out_specs=vmem,
         scratch_shapes=[
             block, block, pltpu.VMEM((groups, tokens), f32),
-            pltpu.VMEM((groups, states), f32), pltpu.VMEM((groups, states), f32),
-            pltpu.VMEM((2, channels, states), f32), pltpu.VMEM((2, channels, states), f32),
+            pltpu.VMEM((groups, states), f32), pltpu.VMEM((groups, states), f32), matrix, matrix,
             pltpu.VMEM((1, channels), f32), pltpu.VMEM((1, features), f32),
-            pltpu.VMEM((features, hidden), bf16), pltpu.VMEM((features, hidden), bf16),
-            pltpu.VMEM((features, 2 * channels), bf16),
+            pltpu.VMEM((features, hidden), bf16), down, down, pltpu.VMEM((features, 2 * channels), bf16),
             wide, wide, wide, wide, wide,
             pltpu.VMEM((8, width), f32), pltpu.VMEM((4, CHUNKS, width), f32),
             pltpu.VMEM((32, 128), f32), pltpu.VMEM((planes, 32, 128), f32), pltpu.VMEM((16, 128), f32),
             block, pltpu.VMEM((channels, 2 * width), bf16), pltpu.VMEM((tokens, 2 * width), bf16),
-            pltpu.VMEM((slots, tokens, channels), bf16), pltpu.VMEM((slots, tokens, channels), bf16),
-            pltpu.VMEM((SIDE, tokens, features // SIDE), bf16), pltpu.VMEM((tokens, 2 * channels), f32),
-            pltpu.VMEM((tokens, hidden), f32), pltpu.VMEM((tokens, hidden), bf16),
-            pltpu.VMEM((4, tokens, channels), bf16), pltpu.VMEM((4, tokens, channels), bf16),
-            pltpu.VMEM((4, tokens, 2 * channels), f32),
-            block, block, block, halves, halves, block, block,
-            dma((13,)), pltpu.SemaphoreType.REGULAR((3,)), dma((4,)), dma((4, 10)),
-            dma((planes,)), dma((planes,)), dma((10,)), dma((10,)),
+            pieces, pieces, pltpu.VMEM((tokens, 2 * channels), f32),
+            pltpu.VMEM((tokens, hidden), f32), pltpu.VMEM((tokens, 128), f32), pltpu.VMEM((tokens, 2 * hidden), bf16),
+            pltpu.VMEM((tokens, SIDE * span), f32), halves, halves, near, near, pltpu.VMEM((2, 2, tokens // 2, span), f32),
+            packs, packs, pltpu.VMEM((2, 2, tokens // 4, span), f32),
+            dma((14,)), pltpu.SemaphoreType.REGULAR((3,)), dma((5,)), dma((5, 8)),
+            dma((planes,)), dma((planes,)), dma((3,)), dma((3,)), dma((2, 3)), dma((2, 4)),
         ],
         name="layer",
         compiler_params=pltpu.CompilerParams(

time: 68.3 us -> 66.8 us (0.978)
  Pallas kernels: 66.6 us -> 65 us
    pallas_call x1, Pallas kernels: 66.6 us -> 65 us  [per_device(): pl.pallas_call(layer_kernel, out_shape=jax.ShapeDtypeStruct((tokens, chan...]
where the time goes in v5:
time: 66.8 us; the launch traced here: 66.7 us
  Pallas kernels  65 us (97%)
  local copies, waits for them, and re-layouts  1.62 us (2%)
    pallas_call x1, Pallas kernels, per_device(): pl.pallas_call(layer_kernel, out_shape=jax.ShapeDtypeStruct((tokens, chan...  65 us
    unnamed x1, local copies, waits for them, and re-layouts  1.62 us

profile of v5, /device:TPU:1, one launch (start us, length us, event | category | flops | bytes accessed | tf_op | source)
XLA Modules:
  0.0 66.7 jit_solution(5837795434116404668)
XLA Ops:
  0.0 65.0 %layer.1 = bf16[384,256]{1,0:T(8,128)(2,1)} custom-call(bf16[384,256]{1,0:T(8,128)(2,1)} %resid_hbm.1, bf16[384,256]{1,0:T(8,128)(2,1)} %u_hbm.1, f32[16,384]{1,0:T(8,128)} %bitcast.9, f32[16,64]{1,0:T(8,128)} %dr_hbm.1, f32[16,64]{1,0:T(8,128)} %fr_hbm.1, f32[2,256,64]{2,1,0:T(8,128)} %bitcast.7, f32[2,256,64]{2,1,0:T(8,128)} %bitcast.8, ...), custom_call_target="tpu_custom_call" | custom-call | tf_op jit(solution)/shard_map/layer/pallas_call | solution.py:809
  65.0 1.6 %copy.15 = bf16[384,256]{1,0:T(8,128)(2,1)} copy(bf16[384,256]{1,0:T(8,128)(2,1)} %layer.1) | data formatting | bytes 393216

commit v6 on v5

--- a/solution.py
+++ b/solution.py
@@ -271,11 +271,10 @@
                 self.send(side, 0, 0, k, 1, 0)
                 self.send(side, 0, 0, 1 - k, -1, 0)
 
-    def send_q(self, dp):
-        for k in range(2):
-            for side in range(2):
-                self.send(side, dp, 0, k, 0, 1)
-                self.send(side, dp, 0, 1 - k, 0, -1)
+    def send_q(self, dp, k):
+        for side in range(2):
+            self.send(side, dp, 0, k, 0, 1)
+            self.send(side, dp, 0, 1 - k, 0, -1)
 
     def forward_p(self):
         self.arrived(0)
@@ -285,12 +284,19 @@
 
     def near(self):
         self.arrived(1)
-        self.send_q(-1)
-        self.send_q(1)
+        self.send_q(-1, 0)
+        self.send_q(1, 0)
+
+    def near_rest(self):
+        self.send_q(-1, 1)
+        self.send_q(1, 1)
 
     def far(self):
         self.arrived(2)
-        self.send_q(2)
+        self.send_q(2, 0)
+
+    def far_rest(self):
+        self.send_q(2, 1)
 
     def forward_q(self, dp):
         self.arrived(3 + dp % SIDE)
@@ -397,7 +403,7 @@
     resid_ref, u_ref, ls_ref, dr_ref, fr_ref, bm_ref, cm_ref, skip_ref, gain_ref,
     up_all, down_first, down_last, vg, dec_re, dec_im, feed_re, feed_im, step_wide, rows, ends, total, totals, carry,
     uperm, wout, states, mixed_all, upd_all, glu, raised, squares, hidden,
-    products, stage_far, relay_in, stage_near, from_near, kept, stage_own, from_own, own_part,
+    products, stage_far, relay_in, stage_near, from_near, kept, stage_own, from_own, own_part, kept_out,
     local_sem, round_sem, ring_send, ring_recv, tot_send, tot_recv, cross_send, cross_recv, sum_send, sum_recv,
 ):
     phase = Phases()
@@ -459,7 +465,8 @@
     pl.semaphore_wait(barrier, 7)
     phase("start_p")
     up.send_p()
-    up.send_q(0)
+    up.send_q(0, 0)
+    up.send_q(0, 1)
     for copy in crossing:
         copy.start()
 
@@ -486,12 +493,12 @@
     chunk_prefix(ends, total)
     pl.semaphore_wait(round_sem.at[2], 4)
 
-    def total_copy(by, slot, target):
+    def total_copy(src, dst, target):
         return pltpu.make_async_remote_copy(
-            src_ref=total,
-            dst_ref=totals.at[slot],
-            send_sem=tot_send.at[by],
-            recv_sem=tot_recv.at[slot],
+            src_ref=src,
+            dst_ref=dst,
+            send_sem=tot_send.at[0],
+            recv_sem=tot_recv.at[0],
             device_id={"sp": target, "tp": lane},
             device_id_type=AXES,
         )
@@ -500,18 +507,23 @@
     for by in range(1, planes):
         @pl.when(here + by < planes)
         def _():
-            total_copy(by, here, lax.rem(here + by, planes)).start()
+            total_copy(total, totals.at[here], lax.rem(here + by, planes)).start()
 
     phase("serve1")
     up.forward_p()
     up.near()
     up.forward_q(0)
+    up.near_rest()
 
     phase("fold")
+
+    for count in range(1, planes):
+        @pl.when(here == count)
+        def _():
+            total_copy(totals.at[:count], totals.at[:count], lax.rem(here + 1, planes)).wait_recv()
 
     def fold(j, value):
         h_re, h_im = value
-        total_copy(0, j, lax.rem(here + 1, planes)).wait_recv()
         a_re, a_im = totals[j, 0:8, :], totals[j, 8:16, :]
         x_re, x_im = totals[j, 16:24, :], totals[j, 24:32, :]
         return a_re * h_re - a_im * h_im + x_re, a_re * h_im + a_im * h_re + x_im
@@ -522,6 +534,7 @@
     carry[8:16, :] = h_im
     phase("serve2")
     up.far()
+    up.far_rest()
     for copy in local[6:9]:
         copy.wait()
     for copy in crossing:
@@ -553,7 +566,8 @@
     phase("serve3")
     up.forward_q(-1)
     up.forward_q(1)
-    first.send_q(0)
+    first.send_q(0, 0)
+    first.send_q(0, 1)
     phase("mix_near")
     mix.near()
     phase("serve4")
@@ -579,6 +593,7 @@
     phase("serve5")
     first.forward_p()
     first.near()
+    first.near_rest()
     last.send_p()
 
     def up_part(chip, start, core=None):
@@ -605,7 +620,9 @@
     phase("serve6")
     first.forward_q(0)
     first.far()
-    last.send_q(0)
+    last.send_q(0, 0)
+    first.far_rest()
+    last.send_q(0, 1)
     phase("upd_near")
     upd.near()
     phase("upd_left")
@@ -636,30 +653,41 @@
     phase("serve9")
     last.far()
     last.forward_q(0)
+    last.near_rest()
+    last.far_rest()
 
     span = piece // 2
     quarter = half // 2
 
-    def low_lanes(rows):
-        return lax.broadcasted_iota(jnp.int32, (rows, span), 1) < span // 2
+    chunk = quarter // 2
 
     def turned(value, by=None):
         return pltpu.roll(value, span // 2 if by is None else by, 1)
 
+    low_lanes = lax.broadcasted_iota(jnp.int32, (chunk, span), 1) < span // 2
+
     def packed(value, core):
-        top, low = value[:quarter], value[quarter:]
-        if core == 0:
-            return jnp.where(low_lanes(quarter), top, turned(low))
-        return jnp.where(low_lanes(quarter), turned(top), low)
+        parts = []
+        for c in range(value.shape[0] // quarter):
+            top, low = (value[c * quarter + k * chunk : c * quarter + k * chunk + chunk] for k in range(2))
+            parts.append(jnp.where(low_lanes, top, turned(low)) if core == 0 else jnp.where(low_lanes, turned(top), low))
+        return jnp.concatenate(parts, axis=0)
 
     class Sum:
         def __init__(self, k, buf):
             self.k, self.buf = k, buf
             self.relays = [
-                self.copy(0, j, stage_far.at[k, j], relay_in.at[k, j], target) for j, target in enumerate((right, left))
+                [
+                    self.copy(
+                        0, 2 * j + c, stage_far.at[k, j, c * quarter : c * quarter + quarter],
+                        relay_in.at[k, j, c * quarter : c * quarter + quarter], target,
+                    )
+                    for c in range(2)
+                ]
+                for j, target in enumerate((right, left))
             ]
-            self.own = self.copy(1, 2, stage_own.at[k], from_own.at[k], partner)
-            self.near = self.copy(2, 3, stage_near.at[k], from_near.at[k], right)
+            self.own = self.copy(1, 4, stage_own.at[k], from_own.at[k], partner)
+            self.near = self.copy(2, 5, stage_near.at[k], from_near.at[k], right)
 
         def copy(self, send, recv, src, dst, target):
             return pltpu.make_async_remote_copy(
@@ -674,13 +702,14 @@
         def product(self, dx):
             return products[:, pl.ds(pl.multiple_of(around(mix.x, dx) * span, span), span)]
 
-        def send_near(self, side, part, value):
+        def send_near(self, side, part, value, first=0):
             chip = around(mix.x, 1 - 2 * side)
+            rows = slice(first, first + value.shape[0] // 2)
             for core in range(2):
-                stage_near[self.k, side, core, part] = packed(value, core).astype(bf16)
+                stage_near[self.k, side, core, part, rows] = packed(value, core).astype(bf16)
                 self.copy(
-                    2, 3, stage_near.at[self.k, side, core, part], from_near.at[self.k, mix.core, side, part],
-                    chip * 2 + core,
+                    2, 5, stage_near.at[self.k, side, core, part, rows],
+                    from_near.at[self.k, mix.core, side, part, rows], chip * 2 + core,
                 ).start()
 
         def start(self, *serve):
@@ -689,7 +718,9 @@
             far = self.product(2).astype(bf16)
             for j in range(2):
                 stage_far[k, j] = far[j * half : j * half + half]
-                self.relays[j].start()
+            for c in range(2):
+                for j in range(2):
+                    self.relays[j][c].start()
             near = self.product(1)
             self.send_near(0, 1, near[half:])
             kept[k, 0] = near[:half]
@@ -708,9 +739,12 @@
                 serve[1]()
 
         def relay(self):
-            for j in range(2):
-                self.relays[j].wait_recv()
-                self.send_near(j, j, kept[self.k, j] + relay_in[self.k, j].astype(f32))
+            k = self.k
+            for c in range(2):
+                rows = slice(c * quarter, c * quarter + quarter)
+                for j in range(2):
+                    self.relays[j][c].wait_recv()
+                    self.send_near(j, j, kept[k, j, rows] + relay_in[k, j, rows].astype(f32), c * chunk)
 
         def result(self):
             k = self.k
@@ -722,7 +756,9 @@
                 for j in range(2):
                     here_part = jnp.where(mix.core == core, own_part[k, j], from_own[k, j].astype(f32))
                     total = here_part + (from_near[k, core, 0, j].astype(f32) + from_near[k, core, 1, j].astype(f32))
-                    rows += [total, turned(total)]
+                    for c in range(2):
+                        part = total[c * chunk : c * chunk + chunk]
+                        rows += [part, turned(part)]
                 found.append(jnp.concatenate(rows, axis=0))
             return found
 
@@ -754,28 +790,31 @@
     phase("last_relay")
     late.relay()
     phase("first_result")
-    one = early.result()
+    lane_group = lax.broadcasted_iota(jnp.int32, (tokens, span), 1) // slim
+    blocks = [upd_all[upd.x, :, own_cols].astype(f32)[:, b * span : b * span + span] for b in range(2)]
+
+    def put_in(k, found):
+        for b in range(2):
+            for core in range(2):
+                place = core * 2 + k
+                moved = turned(found[core], (place - b) % 4 * slim) if place != b else found[core]
+                blocks[b] = blocks[b] + jnp.where(lane_group == place, moved, 0.0)
+
+    put_in(0, early.result())
+    for b in range(2):
+        kept_out[:, b * span : b * span + span] = blocks[b]
     phase("last_result")
     two = late.result()
     phase("result")
-    lane_group = lax.broadcasted_iota(jnp.int32, (tokens, span), 1) // slim
-    blocks = []
-    for b in range(2):
-        block = None
-        for core in range(2):
-            for k, part in enumerate((one[core], two[core])):
-                place = core * 2 + k
-                moved = turned(part, (place - b) % 4 * slim) if place != b else part
-                block = moved if block is None else jnp.where(lane_group == place, moved, block)
-        blocks.append(block)
-    down_sum = jnp.concatenate(blocks, axis=1)
-    out_ref[...] = (upd_all[upd.x, :, own_cols].astype(f32) + down_sum).astype(bf16)
+    blocks = [kept_out[:, b * span : b * span + span] for b in range(2)]
+    put_in(1, two)
+    out_ref[...] = jnp.concatenate(blocks, axis=1).astype(bf16)
 
     phase("drain")
-    for by in range(1, planes):
-        @pl.when(here + by < planes)
+    for count in range(1, planes):
+        @pl.when(planes - 1 - here == count)
         def _():
-            total_copy(by, here, lax.rem(here + by, planes)).wait_send()
+            total_copy(totals.at[:count], totals.at[:count], lax.rem(here + 1, planes)).wait_send()
 
     for part in (up, first, last, mix, upd, early, late):
         part.drain()
@@ -823,9 +862,9 @@
             pieces, pieces, pltpu.VMEM((tokens, 2 * channels), f32),
             pltpu.VMEM((tokens, hidden), f32), pltpu.VMEM((tokens, 128), f32), pltpu.VMEM((tokens, 2 * hidden), bf16),
             pltpu.VMEM((tokens, SIDE * span), f32), halves, halves, near, near, pltpu.VMEM((2, 2, tokens // 2, span), f32),
-            packs, packs, pltpu.VMEM((2, 2, tokens // 4, span), f32),
+            packs, packs, pltpu.VMEM((2, 2, tokens // 4, span), f32), pltpu.VMEM((tokens, channels), f32),
             dma((14,)), pltpu.SemaphoreType.REGULAR((3,)), dma((5,)), dma((5, 8)),
-            dma((planes,)), dma((planes,)), dma((3,)), dma((3,)), dma((2, 3)), dma((2, 4)),
+            dma((1,)), dma((1,)), dma((3,)), dma((3,)), dma((2, 3)), dma((2, 6)),
         ],
         name="layer",
         compiler_params=pltpu.CompilerParams(

time: 66.8 us -> 65.8 us (0.985)
  Pallas kernels: 65 us -> 64.1 us
    pallas_call x1, Pallas kernels: 65 us -> 64.1 us  [per_device(): pl.pallas_call(layer_kernel, out_shape=jax.ShapeDtypeStruct((tokens, chan...]
where the time goes in v6:
time: 65.8 us; the launch traced here: 65.7 us
  Pallas kernels  64.1 us (97%)
  local copies, waits for them, and re-layouts  1.62 us (2%)
    pallas_call x1, Pallas kernels, per_device(): pl.pallas_call(layer_kernel, out_shape=jax.ShapeDtypeStruct((tokens, chan...  64.1 us
    unnamed x1, local copies, waits for them, and re-layouts  1.62 us

profile of v6, /device:TPU:1, one launch (start us, length us, event | category | flops | bytes accessed | tf_op | source)
XLA Modules:
  0.0 65.7 jit_solution(7300134079960382639)
XLA Ops:
  0.0 64.1 %layer.1 = bf16[384,256]{1,0:T(8,128)(2,1)} custom-call(bf16[384,256]{1,0:T(8,128)(2,1)} %resid_hbm.1, bf16[384,256]{1,0:T(8,128)(2,1)} %u_hbm.1, f32[16,384]{1,0:T(8,128)} %bitcast.9, f32[16,64]{1,0:T(8,128)} %dr_hbm.1, f32[16,64]{1,0:T(8,128)} %fr_hbm.1, f32[2,256,64]{2,1,0:T(8,128)} %bitcast.7, f32[2,256,64]{2,1,0:T(8,128)} %bitcast.8, ...), custom_call_target="tpu_custom_call" | custom-call | tf_op jit(solution)/shard_map/layer/pallas_call | solution.py:848
  64.1 1.6 %copy.15 = bf16[384,256]{1,0:T(8,128)(2,1)} copy(bf16[384,256]{1,0:T(8,128)(2,1)} %layer.1) | data formatting | bytes 393216

commit v7 on v6

--- a/solution.py
+++ b/solution.py
@@ -265,11 +265,10 @@
     def arrived(self, group):
         self.whole(32 if group == 7 else 4, group).wait_recv()
 
-    def send_p(self):
-        for k in range(2):
-            for side in range(2):
-                self.send(side, 0, 0, k, 1, 0)
-                self.send(side, 0, 0, 1 - k, -1, 0)
+    def send_p(self, k):
+        for side in range(2):
+            self.send(side, 0, 0, k, 1, 0)
+            self.send(side, 0, 0, 1 - k, -1, 0)
 
     def send_q(self, dp, k):
         for side in range(2):
@@ -464,7 +463,8 @@
     phase("barrier")
     pl.semaphore_wait(barrier, 7)
     phase("start_p")
-    up.send_p()
+    up.send_p(0)
+    up.send_p(1)
     up.send_q(0, 0)
     up.send_q(0, 1)
     for copy in crossing:
@@ -488,6 +488,11 @@
     first_pass(*scan_refs, 0, 2)
     pl.semaphore_wait(round_sem.at[1], 4)
     greet(2)
+    for copy in local[6:9]:
+        copy.wait()
+    for copy in crossing:
+        copy.wait_recv()
+    first.send_p(0)
     first_pass(*scan_refs, 2, 4)
     phase("chunk")
     chunk_prefix(ends, total)
@@ -532,16 +537,12 @@
     h_re, h_im = lax.fori_loop(0, here, fold, (zero, zero))
     carry[0:8, :] = h_re
     carry[8:16, :] = h_im
+    phase("second_pass")
+    second_pass(dec_re, dec_im, feed_re, feed_im, ends, carry, states)
     phase("serve2")
     up.far()
     up.far_rest()
-    for copy in local[6:9]:
-        copy.wait()
-    for copy in crossing:
-        copy.wait_recv()
-    first.send_p()
-    phase("second_pass")
-    second_pass(dec_re, dec_im, feed_re, feed_im, ends, carry, states)
+    first.send_p(1)
     local[9].wait()
     phase("read_out")
     own_cols = mix.cols(mix.core)
@@ -594,7 +595,8 @@
     first.forward_p()
     first.near()
     first.near_rest()
-    last.send_p()
+    last.send_p(0)
+    last.send_p(1)
 
     def up_part(chip, start, core=None):
         if core is None:

time: 65.8 us -> 65.2 us (level)
  Pallas kernels: 64.1 us -> 63.4 us
where the time goes in v7:
time: 65.2 us; the launch traced here: 65.1 us
  Pallas kernels  63.4 us (97%)
  local copies, waits for them, and re-layouts  1.62 us (2%)
    pallas_call x1, Pallas kernels, per_device(): pl.pallas_call(layer_kernel, out_shape=jax.ShapeDtypeStruct((tokens, chan...  63.4 us
    unnamed x1, local copies, waits for them, and re-layouts  1.62 us

profile of v7, /device:TPU:1, one launch (start us, length us, event | category | flops | bytes accessed | tf_op | source)
XLA Modules:
  0.0 65.1 jit_solution(6117023804768958202)
XLA Ops:
  0.0 63.4 %layer.1 = bf16[384,256]{1,0:T(8,128)(2,1)} custom-call(bf16[384,256]{1,0:T(8,128)(2,1)} %resid_hbm.1, bf16[384,256]{1,0:T(8,128)(2,1)} %u_hbm.1, f32[16,384]{1,0:T(8,128)} %bitcast.9, f32[16,64]{1,0:T(8,128)} %dr_hbm.1, f32[16,64]{1,0:T(8,128)} %fr_hbm.1, f32[2,256,64]{2,1,0:T(8,128)} %bitcast.7, f32[2,256,64]{2,1,0:T(8,128)} %bitcast.8, ...), custom_call_target="tpu_custom_call" | custom-call | tf_op jit(solution)/shard_map/layer/pallas_call | solution.py:850
  63.4 1.6 %copy.15 = bf16[384,256]{1,0:T(8,128)(2,1)} copy(bf16[384,256]{1,0:T(8,128)(2,1)} %layer.1) | data formatting | bytes 393216

commit v8 on v7

--- a/solution.py
+++ b/solution.py
@@ -849,7 +849,7 @@
     dma = pltpu.SemaphoreType.DMA
     return pl.pallas_call(
         layer_kernel,
-        out_shape=jax.ShapeDtypeStruct((tokens, channels), bf16),
+        out_shape=pltpu.VMEM((tokens, channels), bf16),
         in_specs=[hbm] * 13,
         out_specs=vmem,
         scratch_shapes=[

time: 65.2 us -> 63.6 us (0.975)
  local copies, waits for them, and re-layouts: 1.62 us -> 0.68 us
    unnamed x1, local copies, waits for them, and re-layouts: 1.62 us -> 0.68 us
    pallas_call x1, Pallas kernels: 63.4 us -> 62.8 us  [per_device(): pl.pallas_call(layer_kernel, out_shape=pltpu.VMEM((tokens, channels), bf1...]
where the time goes in v8:
time: 63.6 us; the launch traced here: 63.5 us
  Pallas kernels  62.8 us (99%)
  local copies, waits for them, and re-layouts  0.68 us (1%)
    pallas_call x1, Pallas kernels, per_device(): pl.pallas_call(layer_kernel, out_shape=pltpu.VMEM((tokens, channels), bf1...  62.8 us

profile of v8, /device:TPU:1, one launch (start us, length us, event | category | flops | bytes accessed | tf_op | source)
XLA Modules:
  0.0 63.5 jit_solution(4031254684424034871)
XLA Ops:
  0.0 62.8 %layer.1 = bf16[384,256]{1,0:T(8,128)(2,1)S(1)} custom-call(bf16[384,256]{1,0:T(8,128)(2,1)} %resid_hbm.1, bf16[384,256]{1,0:T(8,128)(2,1)} %u_hbm.1, f32[16,384]{1,0:T(8,128)} %bitcast.9, f32[16,64]{1,0:T(8,128)} %dr_hbm.1, f32[16,64]{1,0:T(8,128)} %fr_hbm.1, f32[2,256,64]{2,1,0:T(8,128)} %bitcast.7, f32[2,256,64]{2,1,0:T(8,128)} %bitcast.8, ...), custom_call_target="tpu_custom_call" | custom-call | tf_op jit(solution)/shard_map/layer/pallas_call | solution.py:850
  62.8 0.7 %copy.15 = bf16[384,256]{1,0:T(8,128)(2,1)} copy(bf16[384,256]{1,0:T(8,128)(2,1)S(1)} %layer.1) | data formatting | bytes 393216

commit v9 on v8

--- a/solution.py
+++ b/solution.py
@@ -145,7 +145,7 @@
     )
 
 
-def chunk_prefix(ends, total):
+def chunk_prefix(ends, total, total_x, wide_x):
     width = ends.shape[2]
     value = tuple(ends[k] for k in range(4))
     row = lax.broadcasted_iota(jnp.int32, value[0].shape, 0)
@@ -160,7 +160,10 @@
         value = chain(moved(value, by), value)
     for k in range(4):
         for j in range(width // 128):
-            total[8 * k + j : 8 * k + j + 1, :] = value[k][CHUNKS - 1 :, 128 * j : 128 * j + 128]
+            kept = total if k < 2 else wide_x
+            at = 8 * (k % 2) + j
+            kept[at : at + 1, :] = value[k][CHUNKS - 1 :, 128 * j : 128 * j + 128]
+    total_x[...] = wide_x[...].astype(bf16)
     before = moved(value, 1)
     for k in range(4):
         ends[k] = before[k]
@@ -400,7 +403,7 @@
     resid_hbm, u_hbm, ls_hbm, dr_hbm, fr_hbm, bm_hbm, cm_hbm, skip_hbm, gain_hbm, vw_ref, gw_ref, up_ref, down_ref,
     out_ref,
     resid_ref, u_ref, ls_ref, dr_ref, fr_ref, bm_ref, cm_ref, skip_ref, gain_ref,
-    up_all, down_first, down_last, vg, dec_re, dec_im, feed_re, feed_im, step_wide, rows, ends, total, totals, carry,
+    up_all, down_first, down_last, vg, dec_re, dec_im, feed_re, feed_im, step_wide, rows, ends, total, totals, total_x, totals_x, carry,
     uperm, wout, states, mixed_all, upd_all, glu, raised, squares, hidden,
     products, stage_far, relay_in, stage_near, from_near, kept, stage_own, from_own, own_part, kept_out,
     local_sem, round_sem, ring_send, ring_recv, tot_send, tot_recv, cross_send, cross_recv, sum_send, sum_recv,
@@ -495,15 +498,15 @@
     first.send_p(0)
     first_pass(*scan_refs, 2, 4)
     phase("chunk")
-    chunk_prefix(ends, total)
+    chunk_prefix(ends, total, total_x, carry)
     pl.semaphore_wait(round_sem.at[2], 4)
 
-    def total_copy(src, dst, target):
+    def total_copy(k, src, dst, target):
         return pltpu.make_async_remote_copy(
             src_ref=src,
             dst_ref=dst,
-            send_sem=tot_send.at[0],
-            recv_sem=tot_recv.at[0],
+            send_sem=tot_send.at[k],
+            recv_sem=tot_recv.at[k],
             device_id={"sp": target, "tp": lane},
             device_id_type=AXES,
         )
@@ -512,7 +515,8 @@
     for by in range(1, planes):
         @pl.when(here + by < planes)
         def _():
-            total_copy(total, totals.at[here], lax.rem(here + by, planes)).start()
+            for k, (src, dst) in enumerate(((total, totals), (total_x, totals_x))):
+                total_copy(k, src, dst.at[here], lax.rem(here + by, planes)).start()
 
     phase("serve1")
     up.forward_p()
@@ -525,12 +529,14 @@
     for count in range(1, planes):
         @pl.when(here == count)
         def _():
-            total_copy(totals.at[:count], totals.at[:count], lax.rem(here + 1, planes)).wait_recv()
+            for k, part in enumerate((totals, totals_x)):
+                total_copy(k, part.at[:count], part.at[:count], lax.rem(here + 1, planes)).wait_recv()
 
     def fold(j, value):
         h_re, h_im = value
         a_re, a_im = totals[j, 0:8, :], totals[j, 8:16, :]
-        x_re, x_im = totals[j, 16:24, :], totals[j, 24:32, :]
+        x_both = totals_x[j].astype(f32)
+        x_re, x_im = x_both[0:8], x_both[8:16]
         return a_re * h_re - a_im * h_im + x_re, a_re * h_im + a_im * h_re + x_im
 
     zero = jnp.zeros((8, 128), f32)
@@ -816,7 +822,8 @@
     for count in range(1, planes):
         @pl.when(planes - 1 - here == count)
         def _():
-            total_copy(totals.at[:count], totals.at[:count], lax.rem(here + 1, planes)).wait_send()
+            for k, part in enumerate((totals, totals_x)):
+                total_copy(k, part.at[:count], part.at[:count], lax.rem(here + 1, planes)).wait_send()
 
     for part in (up, first, last, mix, upd, early, late):
         part.drain()
@@ -859,14 +866,15 @@
             pltpu.VMEM((features, hidden), bf16), down, down, pltpu.VMEM((features, 2 * channels), bf16),
             wide, wide, wide, wide, wide,
             pltpu.VMEM((8, width), f32), pltpu.VMEM((4, CHUNKS, width), f32),
-            pltpu.VMEM((32, 128), f32), pltpu.VMEM((planes, 32, 128), f32), pltpu.VMEM((16, 128), f32),
+            pltpu.VMEM((16, 128), f32), pltpu.VMEM((planes, 16, 128), f32),
+            pltpu.VMEM((16, 128), bf16), pltpu.VMEM((planes, 16, 128), bf16), pltpu.VMEM((16, 128), f32),
             block, pltpu.VMEM((channels, 2 * width), bf16), pltpu.VMEM((tokens, 2 * width), bf16),
             pieces, pieces, pltpu.VMEM((tokens, 2 * channels), f32),
             pltpu.VMEM((tokens, hidden), f32), pltpu.VMEM((tokens, 128), f32), pltpu.VMEM((tokens, 2 * hidden), bf16),
             pltpu.VMEM((tokens, SIDE * span), f32), halves, halves, near, near, pltpu.VMEM((2, 2, tokens // 2, span), f32),
             packs, packs, pltpu.VMEM((2, 2, tokens // 4, span), f32), pltpu.VMEM((tokens, channels), f32),
             dma((14,)), pltpu.SemaphoreType.REGULAR((3,)), dma((5,)), dma((5, 8)),
-            dma((1,)), dma((1,)), dma((3,)), dma((3,)), dma((2, 3)), dma((2, 6)),
+            dma((2,)), dma((2,)), dma((3,)), dma((3,)), dma((2, 3)), dma((2, 6)),
         ],
         name="layer",
         compiler_params=pltpu.CompilerParams(

time: 63.6 us -> 63 us (level)
  no operation moved by 1% of the time
where the time goes in v9:
time: 63 us; the launch traced here: 62.9 us
  Pallas kernels  62.2 us (99%)
  local copies, waits for them, and re-layouts  0.68 us (1%)
    pallas_call x1, Pallas kernels, per_device(): pl.pallas_call(layer_kernel, out_shape=pltpu.VMEM((tokens, channels), bf1...  62.2 us

profile of v9, /device:TPU:1, one launch (start us, length us, event | category | flops | bytes accessed | tf_op | source)
XLA Modules:
  0.0 62.9 jit_solution(5745943930231297473)
XLA Ops:
  0.0 62.2 %layer.1 = bf16[384,256]{1,0:T(8,128)(2,1)S(1)} custom-call(bf16[384,256]{1,0:T(8,128)(2,1)} %resid_hbm.1, bf16[384,256]{1,0:T(8,128)(2,1)} %u_hbm.1, f32[16,384]{1,0:T(8,128)} %bitcast.9, f32[16,64]{1,0:T(8,128)} %dr_hbm.1, f32[16,64]{1,0:T(8,128)} %fr_hbm.1, f32[2,256,64]{2,1,0:T(8,128)} %bitcast.7, f32[2,256,64]{2,1,0:T(8,128)} %bitcast.8, ...), custom_call_target="tpu_custom_call" | custom-call | tf_op jit(solution)/shard_map/layer/pallas_call | solution.py:857
  62.2 0.7 %copy.15 = bf16[384,256]{1,0:T(8,128)(2,1)} copy(bf16[384,256]{1,0:T(8,128)(2,1)S(1)} %layer.1) | data formatting | bytes 393216

commit v10 on v9

--- a/solution.py
+++ b/solution.py
@@ -646,6 +646,7 @@
     phase("serve8")
     first.forward_q(2)
     last.near()
+    last.send_q(-1, 1)
     phase("upd_far")
     upd.far()
     up_part(far_chip, False, upd.core)
@@ -661,7 +662,7 @@
     phase("serve9")
     last.far()
     last.forward_q(0)
-    last.near_rest()
+    last.send_q(1, 1)
     last.far_rest()
 
     span = piece // 2

time: 63 us -> 63 us (level)
  no operation moved by 1% of the time
where the time goes in v10:
time: 63 us; the launch traced here: 62.9 us
  Pallas kernels  62.3 us (99%)
  local copies, waits for them, and re-layouts  0.68 us (1%)
    pallas_call x1, Pallas kernels, per_device(): pl.pallas_call(layer_kernel, out_shape=pltpu.VMEM((tokens, channels), bf1...  62.3 us

profile of v10, /device:TPU:1, one launch (start us, length us, event | category | flops | bytes accessed | tf_op | source)
XLA Modules:
  0.0 62.9 jit_solution(12418511143256544086)
XLA Ops:
  0.0 62.3 %layer.1 = bf16[384,256]{1,0:T(8,128)(2,1)S(1)} custom-call(bf16[384,256]{1,0:T(8,128)(2,1)} %resid_hbm.1, bf16[384,256]{1,0:T(8,128)(2,1)} %u_hbm.1, f32[16,384]{1,0:T(8,128)} %bitcast.9, f32[16,64]{1,0:T(8,128)} %dr_hbm.1, f32[16,64]{1,0:T(8,128)} %fr_hbm.1, f32[2,256,64]{2,1,0:T(8,128)} %bitcast.7, f32[2,256,64]{2,1,0:T(8,128)} %bitcast.8, ...), custom_call_target="tpu_custom_call" | custom-call | tf_op jit(solution)/shard_map/layer/pallas_call | solution.py:858
  62.3 0.7 %copy.15 = bf16[384,256]{1,0:T(8,128)(2,1)} copy(bf16[384,256]{1,0:T(8,128)(2,1)S(1)} %layer.1) | data formatting | bytes 393216

commit v11 on v10

--- a/solution.py
+++ b/solution.py
@@ -577,11 +577,11 @@
     first.send_q(0, 1)
     phase("mix_near")
     mix.near()
-    phase("serve4")
-    up.forward_q(2)
     phase("mix_left")
     mix.across(-1)
     glu[...] += glu_part(around(mix.x, -1))
+    phase("serve4")
+    up.forward_q(2)
     phase("mix_right")
     mix.across(1)
     glu[...] += glu_part(around(mix.x, 1))

time: 63 us -> 63 us (level)
  no operation moved by 1% of the time
where the time goes in v11:
time: 63 us; the launch traced here: 62.9 us
  Pallas kernels  62.3 us (99%)
  local copies, waits for them, and re-layouts  0.68 us (1%)
    pallas_call x1, Pallas kernels, per_device(): pl.pallas_call(layer_kernel, out_shape=pltpu.VMEM((tokens, channels), bf1...  62.3 us

profile of v11, /device:TPU:1, one launch (start us, length us, event | category | flops | bytes accessed | tf_op | source)
XLA Modules:
  0.0 62.9 jit_solution(17349284423350823353)
XLA Ops:
  0.0 62.3 %layer.1 = bf16[384,256]{1,0:T(8,128)(2,1)S(1)} custom-call(bf16[384,256]{1,0:T(8,128)(2,1)} %resid_hbm.1, bf16[384,256]{1,0:T(8,128)(2,1)} %u_hbm.1, f32[16,384]{1,0:T(8,128)} %bitcast.9, f32[16,64]{1,0:T(8,128)} %dr_hbm.1, f32[16,64]{1,0:T(8,128)} %fr_hbm.1, f32[2,256,64]{2,1,0:T(8,128)} %bitcast.7, f32[2,256,64]{2,1,0:T(8,128)} %bitcast.8, ...), custom_call_target="tpu_custom_call" | custom-call | tf_op jit(solution)/shard_map/layer/pallas_call | solution.py:858
  62.3 0.7 %copy.15 = bf16[384,256]{1,0:T(8,128)(2,1)} copy(bf16[384,256]{1,0:T(8,128)(2,1)S(1)} %layer.1) | data formatting | bytes 393216
